TPU v7x, 32 devices: a whole 2x2x4 slice. The times are simulated.
32 devices in a mesh: kv: 4 (over y, x), tp: 8 (over z, core).
Axes of the slice: x: 2, y: 2, z: 4, core: 2. Of those that a mesh axis runs over, the one named last changes fastest.
Arguments:
- tokens: bfloat16 [64, 4096], P(None, ('kv', 'tp')), may hold values from -6 to 6
- memory: float32 [64, 16, 256, 128], P('kv', 'tp'), may hold values from -6 to 6
- normalizer: float32 [64, 16, 128], P('kv', 'tp'), may hold values from -6 to 6
- stabilizer: float32 [64, 16], P('kv', 'tp'), may hold values from -4 to 4
- first_gain: float32 [4096], replicated, may hold values from 0.1 to 1.9
- first_gate: bfloat16 [4096, 12288], P('kv', 'tp'), may hold values from -0.09375 to 0.09375
- first_up: bfloat16 [4096, 12288], P('kv', 'tp'), may hold values from -0.09375 to 0.09375
- first_down: bfloat16 [12288, 4096], P('tp', 'kv'), may hold values from -0.078125 to 0.078125
- mixer_gain: float32 [4096], replicated, may hold values from 0.1 to 1.9
- query_weight: bfloat16 [4096, 2048], P(None, 'tp'), may hold values from -0.09375 to 0.09375
- key_weight: bfloat16 [4096, 2048], P(None, 'tp'), may hold values from -0.09375 to 0.09375
- value_weight: bfloat16 [4096, 4096], P(None, 'tp'), may hold values from -0.09375 to 0.09375
- input_weight: bfloat16 [4096, 16], replicated, may hold values from -0.09375 to 0.09375
- forget_weight: bfloat16 [4096, 16], replicated, may hold values from -0.09375 to 0.09375
- forget_bias: float32 [16], P('tp'), may hold values from -2 to 4
- output_weight: bfloat16 [4096, 4096], P('tp'), may hold values from -0.09375 to 0.09375
- last_gain: float32 [4096], replicated, may hold values from 0.1 to 1.9
- last_gate: bfloat16 [4096, 12288], P('kv', 'tp'), may hold values from -0.09375 to 0.09375
- last_up: bfloat16 [4096, 12288], P('kv', 'tp'), may hold values from -0.09375 to 0.09375
- last_down: bfloat16 [12288, 4096], P('tp', 'kv'), may hold values from -0.078125 to 0.078125
Outputs:
- result: bfloat16 [64, 4096], P(None, ('kv', 'tp'))
- new_memory: float32 [64, 16, 256, 128], P('kv', 'tp')
- new_normalizer: float32 [64, 16, 128], P('kv', 'tp')
- new_stabilizer: float32 [64, 16], P('kv', 'tp')
All inputs are finite; a program needn't handle non-finite values.
Results may differ from a plain program's by a relative error of at most 0.025.
Values may be sent and summed in bfloat16 or wider, within the bound.
No kernel may reach another device: no remote copies, remote signals or barrier semaphores. Data moves between devices by JAX's collectives and lax.ppermute only.
A program may use at most 128 MiB of HBM per device.

v0:
```python
import jax
import jax.numpy as jnp
from jax import lax
from jax.sharding import PartitionSpec as P

EPS = 1e-06


def hidden_units(gate_acc, up_acc, squares, model_width):
    scale = lax.rsqrt(squares / model_width + EPS)[:, None]
    return (jax.nn.silu(scale * gate_acc) * (scale * up_acc)).astype(jnp.bfloat16)


def gated_block(block, gain, w_gate, w_up, w_down, model_width):
    f32 = jnp.float32
    width = block.shape[1]
    gain_block = lax.dynamic_slice_in_dim(gain, lax.axis_index("kv") * width, width, 0)
    values = block.astype(f32)
    scaled = (values * gain_block).astype(jnp.bfloat16)
    gate_part = jnp.dot(scaled, w_gate, preferred_element_type=f32)
    up_part = jnp.dot(scaled, w_up, preferred_element_type=f32)
    squares = jnp.sum(values * values, axis=1)
    gate_acc, up_acc, sq_total = (
        lax.psum(gate_part.astype(jnp.bfloat16), "kv").astype(jnp.float32),
        lax.psum(up_part.astype(jnp.bfloat16), "kv").astype(jnp.float32),
        lax.psum(squares.astype(jnp.bfloat16), "kv").astype(jnp.float32),
    )
    hidden = hidden_units(gate_acc, up_acc, sq_total, model_width)
    share = lax.psum_scatter(
        lax.dot_general(
            w_down, hidden, (((0,), (1,)), ((), ())), preferred_element_type=f32
        ).astype(jnp.bfloat16),
        "tp",
        scatter_dimension=0,
        tiled=True,
    ).astype(jnp.float32)
    return share.T


def body(
    tokens,
    memory,
    normalizer,
    stabilizer,
    first_gain,
    first_gate,
    first_up,
    first_down,
    mixer_gain,
    query_weight,
    key_weight,
    value_weight,
    input_weight,
    forget_weight,
    forget_bias,
    output_weight,
    last_gain,
    last_gate,
    last_up,
    last_down,
):
    f32 = jnp.float32
    model_width = first_gain.shape[0]
    rows, col_width = tokens.shape
    block = lax.all_gather(tokens, "tp", axis=1, tiled=True)
    first_share = gated_block(block, first_gain, first_gate, first_up, first_down, model_width)
    stream_one = (tokens.astype(f32) + 0.5 * first_share).astype(jnp.bfloat16)
    seq_count, head_count, value_size, key_size = memory.shape
    moved = lax.all_to_all(
        stream_one.reshape(rows, 1, col_width), "kv", split_axis=0, concat_axis=1, tiled=True
    )
    own_rows = lax.all_gather(moved, "tp", axis=2, tiled=True).reshape(seq_count, model_width)
    row_values = own_rows.astype(f32)
    scale = lax.rsqrt(jnp.mean(row_values * row_values, axis=1, keepdims=True) + EPS)
    cell_in = (row_values * mixer_gain).astype(jnp.bfloat16)
    query = (
        scale * jnp.dot(cell_in, query_weight, preferred_element_type=f32) * key_size ** (-0.5)
    ).reshape(seq_count, head_count, key_size)
    key = (scale * jnp.dot(cell_in, key_weight, preferred_element_type=f32)).reshape(
        seq_count, head_count, key_size
    )
    value = (scale * jnp.dot(cell_in, value_weight, preferred_element_type=f32)).reshape(
        seq_count, head_count, value_size
    )
    first_head = lax.axis_index("tp") * head_count
    input_all = scale * jnp.dot(cell_in, input_weight, preferred_element_type=f32)
    forget_all = scale * jnp.dot(cell_in, forget_weight, preferred_element_type=f32)
    input_pre = lax.dynamic_slice_in_dim(input_all, first_head, head_count, 1)
    log_forget = jax.nn.log_sigmoid(
        lax.dynamic_slice_in_dim(forget_all, first_head, head_count, 1) + forget_bias
    )
    carried = log_forget + stabilizer
    new_stabilizer = jnp.maximum(carried, input_pre)
    keep = jnp.exp(carried - new_stabilizer)
    admit = jnp.exp(input_pre - new_stabilizer)
    recalled = jnp.einsum("bhvd,bhd->bhv", memory, query, precision=lax.Precision.HIGHEST)
    match = jnp.sum(query * key, axis=-1)
    numer = keep[..., None] * recalled + (admit * match)[..., None] * value
    denom = keep * jnp.sum(normalizer * query, axis=-1) + admit * match
    cell_out = (
        (numer / jnp.maximum(jnp.abs(denom), 1.0)[..., None])
        .reshape(seq_count, head_count * value_size)
        .astype(jnp.bfloat16)
    )
    new_memory = (
        keep[..., None, None] * memory
        + admit[..., None, None] * value[..., :, None] * key[..., None, :]
    )
    new_normalizer = keep[..., None] * normalizer + admit[..., None] * key
    partial_heads = jnp.dot(cell_out, output_weight, preferred_element_type=f32)
    mixed = lax.psum(partial_heads.astype(jnp.bfloat16), "tp").astype(jnp.float32)
    rows_two = (row_values + mixed).astype(jnp.bfloat16)
    whole_two = lax.all_to_all(rows_two, "kv", split_axis=1, concat_axis=0, tiled=True)
    last_share = gated_block(whole_two, last_gain, last_gate, last_up, last_down, model_width)
    own_columns = lax.dynamic_slice_in_dim(
        whole_two, lax.axis_index("tp") * col_width, col_width, 1
    )
    result = (own_columns.astype(f32) + 0.5 * last_share).astype(jnp.bfloat16)
    return (result, new_memory, new_normalizer, new_stabilizer)


def solution(mesh):
    in_specs = (
        P(None, ("kv", "tp")),
        P("kv", "tp", None, None),
        P("kv", "tp", None),
        P("kv", "tp"),
        P(),
        P("kv", "tp"),
        P("kv", "tp"),
        P("tp", "kv"),
        P(),
        P(None, "tp"),
        P(None, "tp"),
        P(None, "tp"),
        P(),
        P(),
        P("tp"),
        P("tp", None),
        P(),
        P("kv", "tp"),
        P("kv", "tp"),
        P("tp", "kv"),
    )
    out_specs = (
        P(None, ("kv", "tp")),
        P("kv", "tp", None, None),
        P("kv", "tp", None),
        P("kv", "tp"),
    )
    return jax.shard_map(body, mesh=mesh, in_specs=in_specs, out_specs=out_specs, check_vma=False)
```

profile of v0, /device:TPU:0, one launch (start us, length us, event | category | flops | bytes accessed | tf_op | source)
XLA Modules:
  0.0 307.5 jit_solution(12249599025583255382)
XLA Ops:
  7.2 14.9 %all_gather.6 = bf16[64,1024]{1,0:T(8,128)(2,1)S(1)} all-gather(bf16[64,128]{1,0:T(8,128)(2,1)} %param.20), channel_id=1, replica_groups=mesh['kv'=4,'tp'=8] {'tp'}, dimensions={1}, use_global_device_ids=true | all-gather | bytes 147456 | tf_op jit(solution)/shard_map/all_gather | solution.py:65
  23.0 1.3 convolution_convert_fusion.3
  24.3 1.3 convolution_convert_fusion.4
  25.8 10.0 %psum.49 = bf16[64]{0:T(256)(128)(2,1)S(1)} all-reduce(bf16[64]{0:T(256)(128)(2,1)S(1)} %fusion.3), channel_id=1, replica_groups=mesh['kv'=4,'tp'=8] {'kv'}, use_global_device_ids=true, to_apply=%region_1.0 | all-reduce | flops 64 | bytes 256 | tf_op jit(solution)/shard_map/psum | solution.py:26
  35.8 34.0 %all-reduce.10.cloned.1.call-done = (bf16[64,1536]{1,0:T(8,128)(2,1)}, bf16[64,1536]{1,0:T(8,128)(2,1)}) async-done(((bf16[64,1536]{1,0:T(8,128)(2,1)}, bf16[64,1536]{1,0:T(8,128)(2,1)}), (bf16[64,1536]{1,0:T(8,128)(2,1)}, bf16[64,1536]{1,0:T(8,128)(2,1)})) %all-reduce.10.cloned.1.call-update) | async-done | bytes 393232 | tf_op jit(solution)/shard_map/psum | solution.py:25
  69.8 2.8 fusion
  73.5 30.9 %reduce-scatter.7.cloned.1.call-done = bf16[128,64]{1,0:T(8,128)(2,1)} async-done(((bf16[1024,64]{1,0:T(8,128)(2,1)}), bf16[128,64]{1,0:T(8,128)(2,1)}) %reduce-scatter.7.cloned.1.call-update) | async-done | bytes 16400
  107.1 3.7 %all-to-all-start = ((bf16[4,2,1024]{2,1,0:T(2,128)(2,1)}), bf16[4,2,1024]{2,1,0:T(2,128)(2,1)S(1)}, u32[]{:S(2)}, u32[]{:S(2)}) async-start(bf16[4,2,1024]{2,1,0:T(2,128)(2,1)} %reshape.77), calls=%async_computation | async-start | bytes 32768 | tf_op jit(solution)/shard_map/all_to_all | solution.py:69
  110.8 4.7 %all-to-all-done = bf16[4,2,1024]{2,1,0:T(2,128)(2,1)S(1)} async-done(((bf16[4,2,1024]{2,1,0:T(2,128)(2,1)}), bf16[4,2,1024]{2,1,0:T(2,128)(2,1)S(1)}, u32[]{:S(2)}, u32[]{:S(2)}) %all-to-all-start) | async-done | bytes 16416 | tf_op jit(solution)/shard_map/all_to_all | solution.py:69
  115.5 12.8 %all-gather = bf16[16,4,1,1024]{3,0,1,2:T(8,128)(2,1)S(1)} all-gather(bf16[16,4,1,128]{3,0,1,2:T(8,128)(2,1)S(1)} %bitcast.73), channel_id=2, replica_groups=mesh['kv'=4,'tp'=8] {'tp'}, dimensions={3}, use_global_device_ids=true | all-gather | bytes 147456 | tf_op jit(solution)/shard_map/all_gather | solution.py:72
  129.4 1.9 fusion.2
  132.6 3.5 %convolution_multiply_fusion = f32[16,512]{1,0:T(8,128)} fusion(bf16[16,4096]{1,0:T(8,128)(2,1)S(1)} %multiply_convert_fusion.3, bf16[4096,512]{1,0:T(8,128)(2,1)} %param.31, f32[16]{0:T(128)} %copy-done.8), kind=kOutput, calls=%fused_computation.10 | convolution fusion | flops 67117056 | bytes 4358208 | tf_op jit(solution)/shard_map/dot_general | solution.py:82
  136.0 1.4 reshape.63
  137.4 2.6 convolution_multiply_fusion.1
  140.7 1.4 multiply_reduce_fusion.2
  142.2 1.3 copy.76
  143.5 1.3 copy.74
  144.8 1.1 fusion.26
  145.9 1.1 fusion.25
  147.0 1.4 abs_maximum_fusion
  148.7 5.8 %fusion.27 = f32[16,2,1,256]{3,2,1,0:T(1,128)S(1)} fusion(f32[16,2,128,1]{2,3,1,0:T(1,128)} %bitcast.71, f32[16,2,256,128]{3,2,1,0:T(8,128)} %param.21), kind=kOutput, calls=%fused_computation.61 | convolution fusion | flops 12582912 | bytes 4243456 | tf_op jit(solution)/shard_map/bhvd,bhd->bhv/dot_general | solution.py:96
  154.7 1.3 convolution_convert_fusion
  156.1 51.8 %all-reduce.6.cloned.1.call-done = bf16[16,4096]{1,0:T(8,128)(2,1)} async-done(((bf16[16,4096]{1,0:T(8,128)(2,1)}), bf16[16,4096]{1,0:T(8,128)(2,1)}) %all-reduce.6.cloned.1.call-update) | async-done | bytes 131088 | tf_op jit(solution)/shard_map/psum | solution.py:111
  209.5 3.6 %all-to-all-start.1 = ((bf16[16,4,1024]{2,0,1:T(8,128)(2,1)}), bf16[16,4,1024]{2,0,1:T(8,128)(2,1)S(1)}, u32[]{:S(2)}, u32[]{:S(2)}) async-start(bf16[16,4,1024]{2,0,1:T(8,128)(2,1)} %bitcast.63), calls=%async_computation.1 | async-start | bytes 262144 | tf_op jit(solution)/shard_map/all_to_all | solution.py:113
  213.8 4.3 %all-to-all-done.1 = bf16[16,4,1024]{2,0,1:T(8,128)(2,1)S(1)} async-done(((bf16[16,4,1024]{2,0,1:T(8,128)(2,1)}), bf16[16,4,1024]{2,0,1:T(8,128)(2,1)S(1)}, u32[]{:S(2)}, u32[]{:S(2)}) %all-to-all-start.1) | async-done | bytes 131104 | tf_op jit(solution)/shard_map/all_to_all | solution.py:113
  218.2 3.4 %convolution_convert_fusion.1 = bf16[64,1536]{1,0:T(8,128)(2,1)} fusion(bf16[1024,1536]{1,0:T(8,128)(2,1)} %param.38, bf16[64,1024]{1,0:T(8,128)(2,1)S(1)} %bitcast.66, f32[1024]{0:T(1024)S(1)} %dynamic_slice.19), kind=kOutput, calls=%fused_computation.2 | convolution fusion | flops 201621504 | bytes 3477504 | tf_op jit(solution)/shard_map/dot_general | solution.py:21
  221.5 1.3 convolution_convert_fusion.2
  223.1 8.5 %psum.53 = bf16[64]{0:T(256)(128)(2,1)S(1)} all-reduce(bf16[64]{0:T(256)(128)(2,1)S(1)} %convert_element_type.143), channel_id=1, replica_groups=mesh['kv'=4,'tp'=8] {'kv'}, use_global_device_ids=true, to_apply=%region_10.11 | all-reduce | flops 64 | bytes 256 | tf_op jit(solution)/shard_map/psum | solution.py:26
  231.6 33.2 %all-reduce.8.cloned.1.call-done = (bf16[64,1536]{1,0:T(8,128)(2,1)}, bf16[64,1536]{1,0:T(8,128)(2,1)}) async-done(((bf16[64,1536]{1,0:T(8,128)(2,1)}, bf16[64,1536]{1,0:T(8,128)(2,1)}), (bf16[64,1536]{1,0:T(8,128)(2,1)}, bf16[64,1536]{1,0:T(8,128)(2,1)})) %all-reduce.8.cloned.1.call-update) | async-done | bytes 393232 | tf_op jit(solution)/shard_map/psum | solution.py:25
  264.8 2.8 fusion.1
  268.5 4.2 %multiply_add_fusion = f32[16,2,256,128]{3,2,1,0:T(8,128)} fusion(f32[16,2,256,128]{3,2,1,0:T(8,128)} %param.21, f32[16,2,128]{2,1,0:T(2,128)S(1)} %reshape.62, f32[16,2,256]{2,1,0:T(2,128)S(1)} %get-tuple-element.15, f32[16,2]{1,0:T(8,128)S(1)} %copy.73), kind=kLoop, calls=%fused_computation.1 | loop fusion | flops 3145728 | bytes 8437888 | tf_op jit(solution)/shard_map/add | solution.py:106
  273.5 26.0 %reduce-scatter.9.cloned.1.call-done = bf16[128,64]{1,0:T(8,128)(2,1)} async-done(((bf16[1024,64]{1,0:T(8,128)(2,1)}), bf16[128,64]{1,0:T(8,128)(2,1)}) %reduce-scatter.9.cloned.1.call-update) | async-done | bytes 16400
  (65 shorter events, 13.7 us)
Async XLA Ops:
  7.2 15.8 %copy-start = (bf16[1024,1536]{1,0:T(8,128)(2,1)S(1)}, bf16[1024,1536]{1,0:T(8,128)(2,1)}, u32[]{:S(2)}) copy-start(bf16[1024,1536]{1,0:T(8,128)(2,1)} %param.26) | copy-start | bytes 9437188
  7.2 62.6 %all-reduce.10.cloned.1.call-start = ((), (), s32[]{:S(2)}) async-start(), calls=%async_computation.8 | async-start | bytes 786432 | tf_op jit(solution)/shard_map/psum | solution.py:25
  22.1 2.2 copy-start.2
  25.6 79.7 %copy-start.5 = (bf16[64,128]{1,0:T(8,128)(2,1)S(1)}, bf16[64,128]{1,0:T(8,128)(2,1)}, u32[]{:S(2)}) copy-start(bf16[64,128]{1,0:T(8,128)(2,1)} %param.20) | copy-start | bytes 49156
  25.6 78.8 %reduce-scatter.7.cloned.1.call-start = ((), (), s32[]{:S(2)}) async-start(), calls=%async_computation.5 | async-start | bytes 294912
  69.8 59.0 %copy-start.7 = (f32[4096]{0:T(1024)S(1)}, f32[4096]{0:T(1024)}, u32[]{:S(2)}) copy-start(f32[4096]{0:T(1024)} %param.28) | copy-start | bytes 49156
  107.1 8.4 %all-to-all-start = ((bf16[4,2,1024]{2,1,0:T(2,128)(2,1)}), bf16[4,2,1024]{2,1,0:T(2,128)(2,1)S(1)}, u32[]{:S(2)}, u32[]{:S(2)}) async-start(bf16[4,2,1024]{2,1,0:T(2,128)(2,1)} %reshape.77), calls=%async_computation | async-start | bytes 32768 | tf_op jit(solution)/shard_map/all_to_all | solution.py:69
  110.8 97.1 %all-reduce.6.cloned.1.call-start = ((), (), s32[]{:S(2)}) async-start(), calls=%async_computation.4 | async-start | bytes 262144 | tf_op jit(solution)/shard_map/psum | solution.py:111
  128.8 0.6 copy-start.8
  132.6 4.8 %copy-start.9 = (f32[16]{0:T(128)S(1)}, f32[16]{0:T(128)}, u32[]{:S(2)}) copy-start(f32[16]{0:T(128)} %copy-done.8) | copy-start | bytes 196
  147.0 7.6 %copy-start.4 = (f32[16,2,256]{2,1,0:T(2,128)S(1)}, f32[16,2,256]{2,1,0:T(2,128)}, u32[]{:S(2)}) copy-start(f32[16,2,256]{2,1,0:T(2,128)} %reshape.63) | copy-start | bytes 98308
  148.7 6.0 %copy-start.1 = (bf16[512,4096]{1,0:T(8,128)(2,1)S(1)}, bf16[512,4096]{1,0:T(8,128)(2,1)}, u32[]{:S(2)}) copy-start(bf16[512,4096]{1,0:T(8,128)(2,1)} %param.35) | copy-start | bytes 12582916
  209.5 8.7 %all-to-all-start.1 = ((bf16[16,4,1024]{2,0,1:T(8,128)(2,1)}), bf16[16,4,1024]{2,0,1:T(8,128)(2,1)S(1)}, u32[]{:S(2)}, u32[]{:S(2)}) async-start(bf16[16,4,1024]{2,0,1:T(8,128)(2,1)} %bitcast.63), calls=%async_computation.1 | async-start | bytes 262144 | tf_op jit(solution)/shard_map/all_to_all | solution.py:113
  213.1 51.7 %all-reduce.8.cloned.1.call-start = ((), (), s32[]{:S(2)}) async-start(), calls=%async_computation.7 | async-start | bytes 786432 | tf_op jit(solution)/shard_map/psum | solution.py:25
  218.2 3.4 %copy-start.3 = (bf16[1024,1536]{1,0:T(8,128)(2,1)S(1)}, bf16[1024,1536]{1,0:T(8,128)(2,1)}, u32[]{:S(2)}) copy-start(bf16[1024,1536]{1,0:T(8,128)(2,1)} %param.37) | copy-start | bytes 9437188
  222.9 76.6 %reduce-scatter.9.cloned.1.call-start = ((), (), s32[]{:S(2)}) async-start(), calls=%async_computation.6 | async-start | bytes 294912
  268.5 4.2 %copy-start.6 = (f32[16,2,128]{2,1,0:T(2,128)S(1)}, f32[16,2,128]{2,1,0:T(2,128)}, u32[]{:S(2)}) copy-start(f32[16,2,128]{2,1,0:T(2,128)} %param.22) | copy-start | bytes 49156
Sparse Core Ops, SparseCore 0:
  25.7 44.0 all-reduce.9
  73.6 30.7 reduce-scatter.6
  156.2 51.6 all-reduce.5
  223.0 41.7 all-reduce.7
  268.6 30.7 reduce-scatter.8
where the time goes:
time: 308 us; the launch traced here: 307 us
  waiting for transfers between devices  185 us (60%)
  blocking collectives  46.2 us (15%)
  matrix products  30.2 us (10%)
  local copies, waits for them, and re-layouts  14 us (5%)
  between operations  13.9 us (5%)
  other arithmetic  10.6 us (3%)
  starting transfers between devices  7.45 us (2%)
    psum x2, waiting for transfers between devices, gated_block(): lax.psum(up_part.astype(jnp.bfloat16), 'kv').astype(jnp.float32)  67.2 us
    unnamed x7, waiting for transfers between devices  57 us
    psum x1, waiting for transfers between devices, body(): lax.psum(partial_heads.astype(jnp.bfloat16), 'tp').astype(jnp.float32)  51.8 us
    psum x2, blocking collectives, gated_block(): lax.psum(squares.astype(jnp.bfloat16), 'kv').astype(jnp.float32)  18.5 us
    all_gather x1, blocking collectives, body(): block = lax.all_gather(tokens, 'tp', axis=1, tiled=True)  14.9 us
    all_gather x1, blocking collectives, body(): lax.all_gather(moved, 'tp', axis=2, tiled=True)  12.8 us
  transfers between devices with their start and end apart: 7, of which 7 were waited for; matrix products, arithmetic and copies ran while one was open for 2% of the time, Pallas kernels for 0%

commit v1 on v0

v1 whole, which is shorter than its diff:
```python
import jax
import jax.numpy as jnp
from jax import lax
from jax.sharding import PartitionSpec as P

EPS = 1e-06
LANES = 128
F32 = jnp.float32
BF16 = jnp.bfloat16


def shifts(axis):
    size = lax.axis_size(axis)
    return [[(s, (s + d) % size) for s in range(size)] for d in range(1, size)]


def sum_rows_scattered(parts, axis):
    size = lax.axis_size(axis)
    me = lax.axis_index(axis)
    if size > 4:
        got = lax.all_to_all(parts, axis, split_axis=0, concat_axis=0, tiled=True)
        return jnp.sum(got.astype(F32), axis=0)
    total = lax.dynamic_index_in_dim(parts, me, 0, keepdims=False).astype(F32)
    for d, perm in enumerate(shifts(axis), 1):
        piece = lax.dynamic_index_in_dim(parts, (me + d) % size, 0, keepdims=False)
        total = total + lax.ppermute(piece, axis, perm).astype(F32)
    return total


def gather_rows(piece, axis):
    size = lax.axis_size(axis)
    me = lax.axis_index(axis)
    rows = piece.shape[0]
    if size > 4:
        return gather_blocks(piece, axis).reshape(size * rows, piece.shape[1])
    whole = jnp.zeros((size * rows, piece.shape[1]), piece.dtype)
    whole = lax.dynamic_update_slice_in_dim(whole, piece, me * rows, 0)
    for d, perm in enumerate(shifts(axis), 1):
        got = lax.ppermute(piece, axis, perm)
        whole = lax.dynamic_update_slice_in_dim(whole, got, ((me - d) % size) * rows, 0)
    return whole


def gather_blocks(piece, axis):
    size = lax.axis_size(axis)
    return lax.all_to_all(
        jnp.broadcast_to(piece[None], (size,) + piece.shape), axis, 0, 0, tiled=True
    )


def side_by_side(blocks):
    count, rows, cols = blocks.shape
    return jnp.transpose(blocks, (1, 0, 2)).reshape(rows, count * cols)


def apart(whole, count):
    rows, cols = whole.shape
    return jnp.transpose(whole.reshape(rows, count, cols // count), (1, 0, 2))


def gated_share(block, gain, w_gate, w_up, w_down, model_width):
    groups = lax.axis_size("kv")
    rows, width = block.shape
    units = w_gate.shape[1]
    gain_block = lax.dynamic_slice_in_dim(gain, lax.axis_index("kv") * width, width, 0)
    values = block.astype(F32)
    scaled = (values * gain_block).astype(BF16)
    gate = jnp.dot(scaled, w_gate, preferred_element_type=F32).astype(BF16)
    up = jnp.dot(scaled, w_up, preferred_element_type=F32).astype(BF16)
    squares = jnp.sum(values * values, axis=1, keepdims=True)
    high = squares.astype(BF16)
    low = (squares - high.astype(F32)).astype(BF16)
    tail = jnp.concatenate([high, low, jnp.zeros((rows, LANES - 2), BF16)], axis=1)
    parts = jnp.concatenate([gate, up, tail], axis=1).reshape(groups, rows // groups, -1)
    total = sum_rows_scattered(parts, "kv")
    sq = total[:, 2 * units : 2 * units + 1] + total[:, 2 * units + 1 : 2 * units + 2]
    scale = lax.rsqrt(sq / model_width + EPS)
    piece = (jax.nn.silu(scale * total[:, :units]) * (scale * total[:, units : 2 * units])).astype(BF16)
    hidden = gather_rows(piece, "kv")
    sums = jnp.dot(hidden, w_down, preferred_element_type=F32).astype(BF16)
    got = lax.all_to_all(apart(sums, lax.axis_size("tp")), "tp", 0, 0, tiled=True)
    return jnp.sum(got.astype(F32), axis=0)


def body(
    tokens,
    memory,
    normalizer,
    stabilizer,
    first_gain,
    first_gate,
    first_up,
    first_down,
    mixer_gain,
    query_weight,
    key_weight,
    value_weight,
    input_weight,
    forget_weight,
    forget_bias,
    output_weight,
    last_gain,
    last_gate,
    last_up,
    last_down,
):
    model_width = first_gain.shape[0]
    rows, col_width = tokens.shape
    groups, members = lax.axis_size("kv"), lax.axis_size("tp")
    seq_count, head_count, value_size, key_size = memory.shape
    block = side_by_side(gather_blocks(tokens, "tp"))
    share = gated_share(block, first_gain, first_gate, first_up, first_down, model_width)
    stream_one = (tokens.astype(F32) + 0.5 * share).astype(BF16)
    spread = jnp.broadcast_to(
        stream_one.reshape(groups, 1, seq_count, col_width),
        (groups, members, seq_count, col_width),
    ).reshape(groups * members, seq_count, col_width)
    own_rows = side_by_side(lax.all_to_all(spread, ("kv", "tp"), 0, 0, tiled=True))
    row_values = own_rows.astype(F32)
    scale = lax.rsqrt(jnp.mean(row_values * row_values, axis=1, keepdims=True) + EPS)
    cell_in = (row_values * mixer_gain).astype(BF16)
    query = (
        scale * jnp.dot(cell_in, query_weight, preferred_element_type=F32) * key_size ** (-0.5)
    ).reshape(seq_count, head_count, key_size)
    key = (scale * jnp.dot(cell_in, key_weight, preferred_element_type=F32)).reshape(
        seq_count, head_count, key_size
    )
    value = (scale * jnp.dot(cell_in, value_weight, preferred_element_type=F32)).reshape(
        seq_count, head_count, value_size
    )
    first_head = lax.axis_index("tp") * head_count
    gates = scale * jnp.dot(
        cell_in,
        jnp.concatenate(
            [
                lax.dynamic_slice_in_dim(input_weight, first_head, head_count, 1),
                lax.dynamic_slice_in_dim(forget_weight, first_head, head_count, 1),
            ],
            axis=1,
        ),
        preferred_element_type=F32,
    )
    input_pre = gates[:, :head_count]
    log_forget = jax.nn.log_sigmoid(gates[:, head_count:] + forget_bias)
    carried = log_forget + stabilizer
    new_stabilizer = jnp.maximum(carried, input_pre)
    keep = jnp.exp(carried - new_stabilizer)
    admit = jnp.exp(input_pre - new_stabilizer)
    recalled = jnp.sum(memory * query[:, :, None, :], axis=-1)
    match = jnp.sum(query * key, axis=-1)
    numer = keep[..., None] * recalled + (admit * match)[..., None] * value
    denom = keep * jnp.sum(normalizer * query, axis=-1) + admit * match
    cell_out = (
        (numer / jnp.maximum(jnp.abs(denom), 1.0)[..., None])
        .reshape(seq_count, head_count * value_size)
        .astype(BF16)
    )
    new_memory = (
        keep[..., None, None] * memory
        + admit[..., None, None] * value[..., :, None] * key[..., None, :]
    )
    new_normalizer = keep[..., None] * normalizer + admit[..., None] * key
    mixed_part = jnp.dot(cell_out, output_weight, preferred_element_type=F32).astype(BF16)
    pieces = jnp.transpose(
        mixed_part.reshape(seq_count, groups, members, col_width), (2, 1, 0, 3)
    )
    got = lax.all_to_all(pieces, "tp", 0, 0, tiled=True)
    mixed = jnp.sum(got.astype(F32), axis=0)
    held = jnp.transpose(own_rows.reshape(seq_count, groups, members, col_width), (2, 1, 0, 3))
    mine = lax.dynamic_index_in_dim(held, lax.axis_index("tp"), 0, keepdims=False)
    rows_two = (mine.astype(F32) + mixed).astype(BF16)
    spread = jnp.broadcast_to(
        rows_two[:, None], (groups, members, seq_count, col_width)
    ).reshape(groups * members, seq_count, col_width)
    got = lax.all_to_all(spread, ("kv", "tp"), 0, 0, tiled=True)
    whole_two = jnp.transpose(
        got.reshape(groups, members, seq_count, col_width), (0, 2, 1, 3)
    ).reshape(rows, members * col_width)
    last_share = gated_share(whole_two, last_gain, last_gate, last_up, last_down, model_width)
    own_columns = lax.dynamic_index_in_dim(
        got.reshape(groups, members, seq_count, col_width), lax.axis_index("tp"), 1, keepdims=False
    ).reshape(rows, col_width)
    result = (own_columns.astype(F32) + 0.5 * last_share).astype(BF16)
    return (result, new_memory, new_normalizer, new_stabilizer)


def solution(mesh):
    in_specs = (
        P(None, ("kv", "tp")),
        P("kv", "tp", None, None),
        P("kv", "tp", None),
        P("kv", "tp"),
        P(),
        P("kv", "tp"),
        P("kv", "tp"),
        P("tp", "kv"),
        P(),
        P(None, "tp"),
        P(None, "tp"),
        P(None, "tp"),
        P(),
        P(),
        P("tp"),
        P("tp", None),
        P(),
        P("kv", "tp"),
        P("kv", "tp"),
        P("tp", "kv"),
    )
    out_specs = (
        P(None, ("kv", "tp")),
        P("kv", "tp", None, None),
        P("kv", "tp", None),
        P("kv", "tp"),
    )
    return jax.shard_map(body, mesh=mesh, in_specs=in_specs, out_specs=out_specs, check_vma=False)
```

time: 308 us -> 143 us (0.46)
  waiting for transfers between devices: 185 us -> 51.6 us
  blocking collectives: 46.2 us -> 0 us
  starting transfers between devices: 7.45 us -> 39.2 us
  between operations: 13.9 us -> 1.08 us
  matrix products: 30.2 us -> 22.8 us
    psum x3 -> x0, waiting for transfers between devices: 119 us -> none  [the longest x2 67.2 us: gated_block(): lax.psum(up_part.astype(jnp.bfloat16), 'kv').astype(jnp.float32)]
    unnamed x7 -> x0, waiting for transfers between devices: 57 us -> none
    all_to_all x2 -> x6, waiting for transfers between devices: 9.04 us -> 38.7 us  [the longest x2 11.9 us: gated_share(): lax.all_to_all(apart(sums, lax.axis_size('tp')), 'tp', 0, 0, tiled=True)]
    all_gather x2 -> x0, blocking collectives: 27.7 us -> none  [the longest x1 14.9 us: body(): block = lax.all_gather(tokens, 'tp', axis=1, tiled=True)]
    psum x2 -> x0, blocking collectives: 18.5 us -> none  [gated_block(): lax.psum(squares.astype(jnp.bfloat16), 'kv').astype(jnp.float32)]
    ppermute x0 -> x12, starting transfers between devices: none -> 16.8 us  [the longest x6 8.51 us: gather_rows(): got = lax.ppermute(piece, axis, perm)]
    all_to_all x2 -> x6, starting transfers between devices: 7.32 us -> 22.4 us  [the longest x2 6.74 us: gated_share(): lax.all_to_all(apart(sums, lax.axis_size('tp')), 'tp', 0, 0, tiled=True)]
    ppermute x0 -> x12, waiting for transfers between devices: none -> 12.9 us  [the longest x6 7.3 us: sum_rows_scattered(): total = total + lax.ppermute(piece, axis, perm).astype(F32)]
  transfers between devices with their start and end apart: 7 -> 18, of which waited for: 7 -> 17; matrix products, arithmetic and copies ran while one was open for 2% -> 3% of each run, Pallas kernels for 0% -> 0%
where the time goes in v1:
time: 143 us; the launch traced here: 142 us
  waiting for transfers between devices  51.6 us (36%)
  starting transfers between devices  39.2 us (27%)
  matrix products  22.8 us (16%)
  local copies, waits for them, and re-layouts  16.9 us (12%)
  other arithmetic  10.2 us (7%)
    all_to_all x2, waiting for transfers between devices, gated_share(): lax.all_to_all(apart(sums, lax.axis_size('tp')), 'tp', 0, 0, tiled=True)  11.9 us
    ppermute x6, starting transfers between devices, gather_rows(): got = lax.ppermute(piece, axis, perm)  8.51 us
    ppermute x6, starting transfers between devices, sum_rows_scattered(): total = total + lax.ppermute(piece, axis, perm).astype(F32)  8.25 us
    all_to_all x1, waiting for transfers between devices, body(): got = lax.all_to_all(spread, ('kv', 'tp'), 0, 0, tiled=True)  7.46 us
    ppermute x6, waiting for transfers between devices, sum_rows_scattered(): total = total + lax.ppermute(piece, axis, perm).astype(F32)  7.3 us
    all_to_all x2, starting transfers between devices, gated_share(): lax.all_to_all(apart(sums, lax.axis_size('tp')), 'tp', 0, 0, tiled=True)  6.74 us
    all_to_all x1, waiting for transfers between devices, body(): got = lax.all_to_all(pieces, 'tp', 0, 0, tiled=True)  6.66 us
    all_to_all x1, waiting for transfers between devices, body(): lax.all_to_all(spread, ('kv', 'tp'), 0, 0, tiled=True)  6.64 us
  transfers between devices with their start and end apart: 18, of which 17 were waited for; matrix products, arithmetic and copies ran while one was open for 3% of the time, Pallas kernels for 0%

profile of v1, /device:TPU:0, one launch (start us, length us, event | category | flops | bytes accessed | tf_op | source)
XLA Modules:
  0.0 141.9 jit_solution(14249076651135980892)
XLA Ops:
  0.6 1.5 %broadcast_in_dim.8 = bf16[8,64,128]{2,1,0:T(8,128)(2,1)} broadcast(bf16[64,128]{1,0:T(8,128)(2,1)} %param.20), dimensions={1,2} | broadcast | bytes 147456 | tf_op jit(solution)/shard_map/broadcast_in_dim | solution.py:47
  2.2 6.4 %all-to-all-start = ((bf16[8,64,128]{2,1,0:T(8,128)(2,1)}), bf16[8,64,128]{2,1,0:T(8,128)(2,1)S(1)}, u32[]{:S(2)}, u32[]{:S(2)}) async-start(bf16[8,64,128]{2,1,0:T(8,128)(2,1)} %broadcast_in_dim.8), calls=%async_computation | async-start | bytes 262144 | tf_op jit(solution)/shard_map/all_to_all | solution.py:46
  9.2 6.1 %all-to-all-done = bf16[8,64,128]{2,1,0:T(8,128)(2,1)S(1)} async-done(((bf16[8,64,128]{2,1,0:T(8,128)(2,1)}), bf16[8,64,128]{2,1,0:T(8,128)(2,1)S(1)}, u32[]{:S(2)}, u32[]{:S(2)}) %all-to-all-start) | async-done | bytes 131104 | tf_op jit(solution)/shard_map/all_to_all | solution.py:46
  22.7 1.5 %collective-permute-start = (bf16[16,3200]{1,0:T(8,128)(2,1)}, bf16[16,3200]{1,0:T(8,128)(2,1)}, u32[]{:S(2)}, u32[]{:S(2)}) collective-permute-start(bf16[16,3200]{1,0:T(8,128)(2,1)} %get-tuple-element.24), channel_id=1, source_target_pairs={{0,8},{8,16},{16,24},{24,0},{1,9},{9,17},{17,25},{25,1},{2,10},{10... | collective-permute-start | bytes 307208 | tf_op jit(solution)/shard_map/ppermute | solution.py:26
  24.2 1.5 %collective-permute-start.1 = (bf16[16,3200]{1,0:T(8,128)(2,1)}, bf16[16,3200]{1,0:T(8,128)(2,1)}, u32[]{:S(2)}, u32[]{:S(2)}) collective-permute-start(bf16[16,3200]{1,0:T(8,128)(2,1)} %get-tuple-element.26), channel_id=1, source_target_pairs={{0,16},{8,24},{16,0},{24,8},{1,17},{9,25},{17,1},{25,9},{2,18},{10... | collective-permute-start | bytes 307208 | tf_op jit(solution)/shard_map/ppermute | solution.py:26
  25.7 1.4 %collective-permute-start.2 = (bf16[16,3200]{1,0:T(8,128)(2,1)}, bf16[16,3200]{1,0:T(8,128)(2,1)}, u32[]{:S(2)}, u32[]{:S(2)}) collective-permute-start(bf16[16,3200]{1,0:T(8,128)(2,1)} %get-tuple-element.25), channel_id=1, source_target_pairs={{0,24},{8,0},{16,8},{24,16},{1,25},{9,1},{17,9},{25,17},{2,26},{10... | collective-permute-start | bytes 307208 | tf_op jit(solution)/shard_map/ppermute | solution.py:26
  27.1 2.5 %collective-permute-done = bf16[16,3200]{1,0:T(8,128)(2,1)} collective-permute-done((bf16[16,3200]{1,0:T(8,128)(2,1)}, bf16[16,3200]{1,0:T(8,128)(2,1)}, u32[]{:S(2)}, u32[]{:S(2)}) %collective-permute-start) | collective-permute-done | bytes 102432 | tf_op jit(solution)/shard_map/ppermute | solution.py:26
  32.2 1.8 %collective-permute-start.3 = (bf16[16,1536]{1,0:T(8,128)(2,1)S(1)}, bf16[16,1536]{1,0:T(8,128)(2,1)S(1)}, u32[]{:S(2)}, u32[]{:S(2)}) collective-permute-start(bf16[16,1536]{1,0:T(8,128)(2,1)S(1)} %get-tuple-element.16), channel_id=1, source_target_pairs={{0,8},{8,16},{16,24},{24,0},{1,9},{9,17},{17,25},{25,1},{2,10},{10... | collective-permute-start | bytes 147464 | tf_op jit(solution)/shard_map/ppermute | solution.py:39
  39.1 2.5 %fusion = bf16[8,8,8,128]{3,2,1,0:T(8,128)(2,1)S(1)} fusion(bf16[64,1536]{1,0:T(8,128)(2,1)S(1)} %constant_dynamic-update-slice_fusion.4, bf16[1536,1024]{1,0:T(8,128)(2,1)} %param.27), kind=kOutput, calls=%fused_computation.9 | convolution fusion | flops 201392128 | bytes 3473408 | tf_op jit(solution)/shard_map/dot_general | solution.py:80
  42.4 3.4 %all-to-all-start.1 = ((bf16[8,64,128]{2,1,0:T(8,128)(2,1)}), bf16[8,64,128]{2,1,0:T(8,128)(2,1)S(1)}, u32[]{:S(2)}, u32[]{:S(2)}) async-start(bf16[8,64,128]{2,1,0:T(8,128)(2,1)} %bitcast.121), calls=%async_computation.1 | async-start | bytes 262144 | tf_op jit(solution)/shard_map/all_to_all | solution.py:81
  45.7 6.7 %all-to-all-done.1 = bf16[8,64,128]{2,1,0:T(8,128)(2,1)S(1)} async-done(((bf16[8,64,128]{2,1,0:T(8,128)(2,1)}), bf16[8,64,128]{2,1,0:T(8,128)(2,1)S(1)}, u32[]{:S(2)}, u32[]{:S(2)}) %all-to-all-start.1) | async-done | bytes 131104 | tf_op jit(solution)/shard_map/all_to_all | solution.py:81
  53.2 3.4 %all-to-all-start.2 = ((bf16[32,16,128]{2,1,0:T(8,128)(2,1)}), bf16[32,16,128]{2,1,0:T(8,128)(2,1)S(1)}, u32[]{:S(2)}, u32[]{:S(2)}) async-start(bf16[32,16,128]{2,1,0:T(8,128)(2,1)} %bitcast.9), calls=%async_computation.2 | async-start | bytes 262144 | tf_op jit(solution)/shard_map/all_to_all | solution.py:118
  56.6 1.5 %constant_dynamic-slice_fusion.1 = (bf16[4096,2]{0,1:T(2,128)(2,1)S(1)}, bf16[4096,2]{0,1:T(2,128)(2,1)}) fusion(bf16[4096,16]{0,1:T(8,128)(2,1)} %param.33, s32[]{:T(128)S(6)} %select_n.107, bf16[4096,16]{0,1:T(8,128)(2,1)} %param.32), kind=kLoop, calls=%fused_computation.88 | loop fusion | bytes 65540 | tf_op jit(solution)/shard_map/dynamic_slice | solution.py:137
  58.1 6.6 %all-to-all-done.2 = bf16[32,16,128]{2,1,0:T(8,128)(2,1)S(1)} async-done(((bf16[32,16,128]{2,1,0:T(8,128)(2,1)}), bf16[32,16,128]{2,1,0:T(8,128)(2,1)S(1)}, u32[]{:S(2)}, u32[]{:S(2)}) %all-to-all-start.2) | async-done | bytes 131104 | tf_op jit(solution)/shard_map/all_to_all | solution.py:118
  65.2 2.8 %convolution_multiply_fusion = f32[16,512]{1,0:T(8,128)S(1)} fusion(bf16[16,4096]{1,0:T(8,128)(2,1)S(1)} %fusion.7, bf16[4096,512]{1,0:T(8,128)(2,1)} %param.31, f32[16]{0:T(128)S(1)} %add_rsqrt_fusion), kind=kOutput, calls=%fused_computation.12 | convolution fusion | flops 67117056 | bytes 4358208 | tf_op jit(solution)/shard_map/dot_general | solution.py:128
  68.0 1.9 %convolution_multiply_fusion.1 = f32[16,256]{1,0:T(8,128)S(1)} fusion(bf16[16,4096]{1,0:T(8,128)(2,1)S(1)} %fusion.7, bf16[4096,256]{1,0:T(8,128)(2,1)} %param.30, f32[16]{0:T(128)S(1)} %add_rsqrt_fusion), kind=kOutput, calls=%fused_computation.13 | convolution fusion | flops 33558528 | bytes 2244672 | tf_op jit(solution)/shard_map/dot_general | solution.py:125
  70.0 1.9 %fusion.3 = f32[16,256]{1,0:T(8,128)S(1)} fusion(bf16[16,4096]{1,0:T(8,128)(2,1)S(1)} %fusion.7, bf16[4096,256]{1,0:T(8,128)(2,1)} %param.29, f32[16]{0:T(128)} %copy-done.14), kind=kOutput, calls=%fused_computation.15 | convolution fusion | flops 33562624 | bytes 2244672 | tf_op jit(solution)/shard_map/dot_general | solution.py:123
  74.8 4.8 %multiply_add_fusion = (f32[16,2,256,128]{3,2,1,0:T(8,128)}, f32[16,2,256]{2,1,0:T(2,128)S(1)}) fusion(f32[16,2,256,128]{3,2,1,0:T(8,128)} %param.21, f32[16,2,128]{2,1,0:T(2,128)S(1)} %reshape.176, f32[16,2,256]{2,1,0:T(2,128)S(1)} %broadcast_multiply_fusion, f32[16,2]{1,0:T(8,128)S(1)} %copy.121, f32[16,2,128]{2,1,0:T(2,128)S(1)} %mul.270), kind=kLoop, calls=%fused_computation.1 | loop fusion | flops 5234688 | bytes 8487040 | tf_op jit(solution)/shard_map/add | solution.py:159
  80.1 2.8 %fusion.2 = bf16[2,8,32,128]{3,1,2,0:T(8,128)(2,1)S(1)} fusion(bf16[512,4096]{1,0:T(8,128)(2,1)} %param.35, f32[16,512]{1,0:T(8,128)S(1)} %bitcast.136, f32[16,512]{1,0:T(8,128)S(1)} %bitcast.134, f32[16,512]{1,0:T(8,128)S(1)} %bitcast.135, f32[16,512]{1,0:T(8,128)S(1)} %convolution_multiply_fusion), kind=kOutput, calls=%fused_computation.11 | convolution fusion | flops 67207168 | bytes 4456448 | tf_op jit(solution)/shard_map/dot_general | solution.py:163
  83.7 3.4 %all-to-all-start.3 = ((bf16[8,4,16,128]{3,1,2,0:T(4,128)(2,1)}), bf16[8,4,16,128]{3,1,2,0:T(4,128)(2,1)S(1)}, u32[]{:S(2)}, u32[]{:S(2)}) async-start(bf16[8,4,16,128]{3,1,2,0:T(4,128)(2,1)} %bitcast.122), calls=%async_computation.3 | async-start | bytes 262144 | tf_op jit(solution)/shard_map/all_to_all | solution.py:167
  87.1 6.7 %all-to-all-done.3 = bf16[8,4,16,128]{3,1,2,0:T(4,128)(2,1)S(1)} async-done(((bf16[8,4,16,128]{3,1,2,0:T(4,128)(2,1)}), bf16[8,4,16,128]{3,1,2,0:T(4,128)(2,1)S(1)}, u32[]{:S(2)}, u32[]{:S(2)}) %all-to-all-start.3) | async-done | bytes 131104 | tf_op jit(solution)/shard_map/all_to_all | solution.py:167
  94.5 2.6 %all-to-all-start.4 = ((bf16[32,16,128]{2,1,0:T(8,128)(2,1)}), bf16[32,16,128]{2,1,0:T(8,128)(2,1)S(1)}, u32[]{:S(2)}, u32[]{:S(2)}) async-start(bf16[32,16,128]{2,1,0:T(8,128)(2,1)} %bitcast.16), calls=%async_computation.4 | async-start | bytes 262144 | tf_op jit(solution)/shard_map/all_to_all | solution.py:175
  97.8 7.5 %all-to-all-done.4 = bf16[32,16,128]{2,1,0:T(8,128)(2,1)S(1)} async-done(((bf16[32,16,128]{2,1,0:T(8,128)(2,1)}), bf16[32,16,128]{2,1,0:T(8,128)(2,1)S(1)}, u32[]{:S(2)}, u32[]{:S(2)}) %all-to-all-start.4) | async-done | bytes 131104 | tf_op jit(solution)/shard_map/all_to_all | solution.py:175
  105.4 3.4 %convolution_convert_fusion.1 = bf16[64,1536]{1,0:T(8,128)(2,1)} fusion(bf16[1024,1536]{1,0:T(8,128)(2,1)} %param.38, f32[8,8,8,128]{3,2,1,0:T(8,128)S(1)} %bitcast.123, f32[1024]{0:T(1024)S(1)} %dynamic_slice.54), kind=kOutput, calls=%fused_computation.3 | convolution fusion | flops 201555968 | bytes 3608576 | tf_op jit(solution)/shard_map/dot_general | solution.py:69
  114.4 2.2 %collective-permute-start.8 = (bf16[16,3200]{1,0:T(8,128)(2,1)S(1)}, bf16[16,3200]{1,0:T(8,128)(2,1)S(1)}, u32[]{:S(2)}, u32[]{:S(2)}) collective-permute-start(bf16[16,3200]{1,0:T(8,128)(2,1)S(1)} %get-tuple-element.22), channel_id=1, source_target_pairs={{0,24},{8,0},{16,8},{24,16},{1,25},{9,1},{17,9},{25,17},{2,26},{10... | collective-permute-start | bytes 307208 | tf_op jit(solution)/shard_map/ppermute | solution.py:26
  116.6 2.9 %collective-permute-done.6 = bf16[16,3200]{1,0:T(8,128)(2,1)S(1)} collective-permute-done((bf16[16,3200]{1,0:T(8,128)(2,1)S(1)}, bf16[16,3200]{1,0:T(8,128)(2,1)S(1)}, u32[]{:S(2)}, u32[]{:S(2)}) %collective-permute-start.6) | collective-permute-done | bytes 102432 | tf_op jit(solution)/shard_map/ppermute | solution.py:26
  120.7 1.8 %collective-permute-start.9 = (bf16[16,1536]{1,0:T(8,128)(2,1)S(1)}, bf16[16,1536]{1,0:T(8,128)(2,1)S(1)}, u32[]{:S(2)}, u32[]{:S(2)}) collective-permute-start(bf16[16,1536]{1,0:T(8,128)(2,1)S(1)} %get-tuple-element.7), channel_id=1, source_target_pairs={{0,8},{8,16},{16,24},{24,0},{1,9},{9,17},{17,25},{25,1},{2,10},{10... | collective-permute-start | bytes 147464 | tf_op jit(solution)/shard_map/ppermute | solution.py:39
  122.5 1.4 collective-permute-start.10
  126.6 1.3 collective-permute-done.11
  128.0 2.5 %fusion.1 = bf16[8,8,8,128]{3,2,1,0:T(8,128)(2,1)S(1)} fusion(bf16[64,1536]{1,0:T(8,128)(2,1)S(1)} %constant_dynamic-update-slice_fusion, bf16[1536,1024]{1,0:T(8,128)(2,1)} %param.39), kind=kOutput, calls=%fused_computation.10 | convolution fusion | flops 201392128 | bytes 3473408 | tf_op jit(solution)/shard_map/dot_general | solution.py:80
  131.2 3.4 %all-to-all-start.5 = ((bf16[8,64,128]{2,1,0:T(8,128)(2,1)}), bf16[8,64,128]{2,1,0:T(8,128)(2,1)S(1)}, u32[]{:S(2)}, u32[]{:S(2)}) async-start(bf16[8,64,128]{2,1,0:T(8,128)(2,1)} %bitcast.119), calls=%async_computation.5 | async-start | bytes 262144 | tf_op jit(solution)/shard_map/all_to_all | solution.py:81
  136.0 5.2 %all-to-all-done.5 = bf16[8,64,128]{2,1,0:T(8,128)(2,1)S(1)} async-done(((bf16[8,64,128]{2,1,0:T(8,128)(2,1)}), bf16[8,64,128]{2,1,0:T(8,128)(2,1)S(1)}, u32[]{:S(2)}, u32[]{:S(2)}) %all-to-all-start.5) | async-done | bytes 131104 | tf_op jit(solution)/shard_map/all_to_all | solution.py:81
  (118 shorter events, 35.4 us)
Async XLA Ops:
  0.6 16.3 %copy-start = (bf16[1024,1536]{1,0:T(8,128)(2,1)S(1)}, bf16[1024,1536]{1,0:T(8,128)(2,1)}, u32[]{:S(2)}) copy-start(bf16[1024,1536]{1,0:T(8,128)(2,1)} %param.25) | copy-start | bytes 9437188
  2.2 13.1 %all-to-all-start = ((bf16[8,64,128]{2,1,0:T(8,128)(2,1)}), bf16[8,64,128]{2,1,0:T(8,128)(2,1)S(1)}, u32[]{:S(2)}, u32[]{:S(2)}) async-start(bf16[8,64,128]{2,1,0:T(8,128)(2,1)} %broadcast_in_dim.8), calls=%async_computation | async-start | bytes 262144 | tf_op jit(solution)/shard_map/all_to_all | solution.py:46
  22.7 6.9 %collective-permute-start = (bf16[16,3200]{1,0:T(8,128)(2,1)}, bf16[16,3200]{1,0:T(8,128)(2,1)}, u32[]{:S(2)}, u32[]{:S(2)}) collective-permute-start(bf16[16,3200]{1,0:T(8,128)(2,1)} %get-tuple-element.24), channel_id=1, source_target_pairs={{0,8},{8,16},{16,24},{24,0},{1,9},{9,17},{17,25},{25,1},{2,10},{10... | collective-permute-start | bytes 307208 | tf_op jit(solution)/shard_map/ppermute | solution.py:26
  24.2 6.2 %collective-permute-start.1 = (bf16[16,3200]{1,0:T(8,128)(2,1)}, bf16[16,3200]{1,0:T(8,128)(2,1)}, u32[]{:S(2)}, u32[]{:S(2)}) collective-permute-start(bf16[16,3200]{1,0:T(8,128)(2,1)} %get-tuple-element.26), channel_id=1, source_target_pairs={{0,16},{8,24},{16,0},{24,8},{1,17},{9,25},{17,1},{25,9},{2,18},{10... | collective-permute-start | bytes 307208 | tf_op jit(solution)/shard_map/ppermute | solution.py:26
  25.7 5.1 %collective-permute-start.2 = (bf16[16,3200]{1,0:T(8,128)(2,1)}, bf16[16,3200]{1,0:T(8,128)(2,1)}, u32[]{:S(2)}, u32[]{:S(2)}) collective-permute-start(bf16[16,3200]{1,0:T(8,128)(2,1)} %get-tuple-element.25), channel_id=1, source_target_pairs={{0,24},{8,0},{16,8},{24,16},{1,25},{9,1},{17,9},{25,17},{2,26},{10... | collective-permute-start | bytes 307208 | tf_op jit(solution)/shard_map/ppermute | solution.py:26
  31.9 20.6 %copy-start.10 = (bf16[64,128]{1,0:T(8,128)(2,1)S(1)}, bf16[64,128]{1,0:T(8,128)(2,1)}, u32[]{:S(2)}) copy-start(bf16[64,128]{1,0:T(8,128)(2,1)} %param.20) | copy-start | bytes 49156
  31.9 33.1 %copy-start.13 = (f32[4096]{0:T(1024)S(1)}, f32[4096]{0:T(1024)}, u32[]{:S(2)}) copy-start(f32[4096]{0:T(1024)} %param.28) | copy-start | bytes 49156
  32.2 5.0 %collective-permute-start.3 = (bf16[16,1536]{1,0:T(8,128)(2,1)S(1)}, bf16[16,1536]{1,0:T(8,128)(2,1)S(1)}, u32[]{:S(2)}, u32[]{:S(2)}) collective-permute-start(bf16[16,1536]{1,0:T(8,128)(2,1)S(1)} %get-tuple-element.16), channel_id=1, source_target_pairs={{0,8},{8,16},{16,24},{24,0},{1,9},{9,17},{17,25},{25,1},{2,10},{10... | collective-permute-start | bytes 147464 | tf_op jit(solution)/shard_map/ppermute | solution.py:39
  34.0 4.1 %collective-permute-start.4 = (bf16[16,1536]{1,0:T(8,128)(2,1)S(1)}, bf16[16,1536]{1,0:T(8,128)(2,1)S(1)}, u32[]{:S(2)}, u32[]{:S(2)}) collective-permute-start(bf16[16,1536]{1,0:T(8,128)(2,1)S(1)} %get-tuple-element.16), channel_id=1, source_target_pairs={{0,16},{8,24},{16,0},{24,8},{1,17},{9,25},{17,1},{25,9},{2,18},{10... | collective-permute-start | bytes 147464 | tf_op jit(solution)/shard_map/ppermute | solution.py:39
  35.0 4.1 %collective-permute-start.5 = (bf16[16,1536]{1,0:T(8,128)(2,1)S(1)}, bf16[16,1536]{1,0:T(8,128)(2,1)S(1)}, u32[]{:S(2)}, u32[]{:S(2)}) collective-permute-start(bf16[16,1536]{1,0:T(8,128)(2,1)S(1)} %get-tuple-element.16), channel_id=1, source_target_pairs={{0,24},{8,0},{16,8},{24,16},{1,25},{9,1},{17,9},{25,17},{2,26},{10... | collective-permute-start | bytes 147464 | tf_op jit(solution)/shard_map/ppermute | solution.py:39
  42.4 10.1 %all-to-all-start.1 = ((bf16[8,64,128]{2,1,0:T(8,128)(2,1)}), bf16[8,64,128]{2,1,0:T(8,128)(2,1)S(1)}, u32[]{:S(2)}, u32[]{:S(2)}) async-start(bf16[8,64,128]{2,1,0:T(8,128)(2,1)} %bitcast.121), calls=%async_computation.1 | async-start | bytes 262144 | tf_op jit(solution)/shard_map/all_to_all | solution.py:81
  53.2 11.6 %all-to-all-start.2 = ((bf16[32,16,128]{2,1,0:T(8,128)(2,1)}), bf16[32,16,128]{2,1,0:T(8,128)(2,1)S(1)}, u32[]{:S(2)}, u32[]{:S(2)}) async-start(bf16[32,16,128]{2,1,0:T(8,128)(2,1)} %bitcast.9), calls=%async_computation.2 | async-start | bytes 262144 | tf_op jit(solution)/shard_map/all_to_all | solution.py:118
  64.9 3.1 %copy-start.14 = (f32[16]{0:T(128)}, f32[16]{0:T(128)S(1)}, u32[]{:S(2)}) copy-start(f32[16]{0:T(128)S(1)} %add_rsqrt_fusion) | copy-start | bytes 196
  68.0 4.1 %copy-start.11 = (f32[16,2,128]{2,1,0:T(2,128)S(1)}, f32[16,2,128]{2,1,0:T(2,128)}, u32[]{:S(2)}) copy-start(f32[16,2,128]{2,1,0:T(2,128)} %param.22) | copy-start | bytes 49156
  70.0 9.6 %copy-start.4 = (f32[16,2,128]{2,1,0:T(2,128)}, f32[16,2,128]{2,1,0:T(2,128)S(1)}, u32[]{:S(2)}) copy-start(f32[16,2,128]{2,1,0:T(2,128)S(1)} %reshape.176) | copy-start | bytes 49156
  74.6 5.0 %copy-start.8 = (f32[16,2]{1,0:T(8,128)}, f32[16,2]{1,0:T(8,128)S(1)}, u32[]{:S(2)}) copy-start(f32[16,2]{1,0:T(8,128)S(1)} %copy.133) | copy-start | bytes 388
  74.7 4.9 %copy-start.6 = (f32[16,2]{1,0:T(8,128)}, f32[16,2]{1,0:T(8,128)S(1)}, u32[]{:S(2)}) copy-start(f32[16,2]{1,0:T(8,128)S(1)} %copy.121) | copy-start | bytes 388
  83.7 10.1 %all-to-all-start.3 = ((bf16[8,4,16,128]{3,1,2,0:T(4,128)(2,1)}), bf16[8,4,16,128]{3,1,2,0:T(4,128)(2,1)S(1)}, u32[]{:S(2)}, u32[]{:S(2)}) async-start(bf16[8,4,16,128]{3,1,2,0:T(4,128)(2,1)} %bitcast.122), calls=%async_computation.3 | async-start | bytes 262144 | tf_op jit(solution)/shard_map/all_to_all | solution.py:167
  94.5 10.7 %all-to-all-start.4 = ((bf16[32,16,128]{2,1,0:T(8,128)(2,1)}), bf16[32,16,128]{2,1,0:T(8,128)(2,1)S(1)}, u32[]{:S(2)}, u32[]{:S(2)}) async-start(bf16[32,16,128]{2,1,0:T(8,128)(2,1)} %bitcast.16), calls=%async_computation.4 | async-start | bytes 262144 | tf_op jit(solution)/shard_map/all_to_all | solution.py:175
  105.3 4.8 %copy-start.3 = (bf16[32,16,128]{2,1,0:T(8,128)(2,1)}, bf16[32,16,128]{2,1,0:T(8,128)(2,1)S(1)}, u32[]{:S(2)}) copy-start(bf16[32,16,128]{2,1,0:T(8,128)(2,1)S(1)} %all-to-all-done.4) | copy-start | bytes 393220
  105.3 3.5 %copy-start.2 = (bf16[1024,1536]{1,0:T(8,128)(2,1)S(1)}, bf16[1024,1536]{1,0:T(8,128)(2,1)}, u32[]{:S(2)}) copy-start(bf16[1024,1536]{1,0:T(8,128)(2,1)} %param.37) | copy-start | bytes 9437188
  112.8 6.8 %collective-permute-start.6 = (bf16[16,3200]{1,0:T(8,128)(2,1)S(1)}, bf16[16,3200]{1,0:T(8,128)(2,1)S(1)}, u32[]{:S(2)}, u32[]{:S(2)}) collective-permute-start(bf16[16,3200]{1,0:T(8,128)(2,1)S(1)} %get-tuple-element.21), channel_id=1, source_target_pairs={{0,8},{8,16},{16,24},{24,0},{1,9},{9,17},{17,25},{25,1},{2,10},{10... | collective-permute-start | bytes 307208 | tf_op jit(solution)/shard_map/ppermute | solution.py:26
  113.7 6.6 %collective-permute-start.7 = (bf16[16,3200]{1,0:T(8,128)(2,1)S(1)}, bf16[16,3200]{1,0:T(8,128)(2,1)S(1)}, u32[]{:S(2)}, u32[]{:S(2)}) collective-permute-start(bf16[16,3200]{1,0:T(8,128)(2,1)S(1)} %get-tuple-element.23), channel_id=1, source_target_pairs={{0,16},{8,24},{16,0},{24,8},{1,17},{9,25},{17,1},{25,9},{2,18},{10... | collective-permute-start | bytes 307208 | tf_op jit(solution)/shard_map/ppermute | solution.py:26
  114.4 5.8 %collective-permute-start.8 = (bf16[16,3200]{1,0:T(8,128)(2,1)S(1)}, bf16[16,3200]{1,0:T(8,128)(2,1)S(1)}, u32[]{:S(2)}, u32[]{:S(2)}) collective-permute-start(bf16[16,3200]{1,0:T(8,128)(2,1)S(1)} %get-tuple-element.22), channel_id=1, source_target_pairs={{0,24},{8,0},{16,8},{24,16},{1,25},{9,1},{17,9},{25,17},{2,26},{10... | collective-permute-start | bytes 307208 | tf_op jit(solution)/shard_map/ppermute | solution.py:26
  120.3 14.3 %copy-start.5 = (f32[16,2,128]{2,1,0:T(2,128)S(1)}, f32[16,2,128]{2,1,0:T(2,128)}, u32[]{:S(2)}) copy-start(f32[16,2,128]{2,1,0:T(2,128)} %copy-done.4) | copy-start | bytes 49156
  120.3 14.3 %copy-start.7 = (f32[16,2]{1,0:T(8,128)S(1)}, f32[16,2]{1,0:T(8,128)}, u32[]{:S(2)}) copy-start(f32[16,2]{1,0:T(8,128)} %copy-done.6) | copy-start | bytes 388
  120.3 14.3 %copy-start.9 = (f32[16,2]{1,0:T(8,128)S(1)}, f32[16,2]{1,0:T(8,128)}, u32[]{:S(2)}) copy-start(f32[16,2]{1,0:T(8,128)} %copy-done.8) | copy-start | bytes 388
  120.3 14.3 %copy-start.12 = (f32[16,2,128]{2,1,0:T(2,128)S(1)}, f32[16,2,128]{2,1,0:T(2,128)}, u32[]{:S(2)}) copy-start(f32[16,2,128]{2,1,0:T(2,128)} %param.22) | copy-start | bytes 49156
  120.7 5.2 %collective-permute-start.9 = (bf16[16,1536]{1,0:T(8,128)(2,1)S(1)}, bf16[16,1536]{1,0:T(8,128)(2,1)S(1)}, u32[]{:S(2)}, u32[]{:S(2)}) collective-permute-start(bf16[16,1536]{1,0:T(8,128)(2,1)S(1)} %get-tuple-element.7), channel_id=1, source_target_pairs={{0,8},{8,16},{16,24},{24,0},{1,9},{9,17},{17,25},{25,1},{2,10},{10... | collective-permute-start | bytes 147464 | tf_op jit(solution)/shard_map/ppermute | solution.py:39
  122.5 4.1 %collective-permute-start.10 = (bf16[16,1536]{1,0:T(8,128)(2,1)S(1)}, bf16[16,1536]{1,0:T(8,128)(2,1)S(1)}, u32[]{:S(2)}, u32[]{:S(2)}) collective-permute-start(bf16[16,1536]{1,0:T(8,128)(2,1)S(1)} %get-tuple-element.7), channel_id=1, source_target_pairs={{0,16},{8,24},{16,0},{24,8},{1,17},{9,25},{17,1},{25,9},{2,18},{10... | collective-permute-start | bytes 147464 | tf_op jit(solution)/shard_map/ppermute | solution.py:39
  123.9 4.1 %collective-permute-start.11 = (bf16[16,1536]{1,0:T(8,128)(2,1)S(1)}, bf16[16,1536]{1,0:T(8,128)(2,1)S(1)}, u32[]{:S(2)}, u32[]{:S(2)}) collective-permute-start(bf16[16,1536]{1,0:T(8,128)(2,1)S(1)} %get-tuple-element.7), channel_id=1, source_target_pairs={{0,24},{8,0},{16,8},{24,16},{1,25},{9,1},{17,9},{25,17},{2,26},{10... | collective-permute-start | bytes 147464 | tf_op jit(solution)/shard_map/ppermute | solution.py:39
  131.2 10.1 %all-to-all-start.5 = ((bf16[8,64,128]{2,1,0:T(8,128)(2,1)}), bf16[8,64,128]{2,1,0:T(8,128)(2,1)S(1)}, u32[]{:S(2)}, u32[]{:S(2)}) async-start(bf16[8,64,128]{2,1,0:T(8,128)(2,1)} %bitcast.119), calls=%async_computation.5 | async-start | bytes 262144 | tf_op jit(solution)/shard_map/all_to_all | solution.py:81
  (1 other events, 2.0 us)

commit v2 on v1

v2 whole, which is shorter than its diff:
```python
import jax
import jax.numpy as jnp
from jax import lax
from jax.experimental import pallas as pl
from jax.experimental.pallas import tpu as pltpu
from jax.sharding import PartitionSpec as P

EPS = 1e-06
LANES = 128
F32 = jnp.float32
BF16 = jnp.bfloat16


def shifts(axis):
    size = lax.axis_size(axis)
    return [[(s, (s + d) % size) for s in range(size)] for d in range(1, size)]


def sum_rows_scattered(parts, axis):
    size = lax.axis_size(axis)
    me = lax.axis_index(axis)
    if size > 4:
        got = lax.all_to_all(parts, axis, split_axis=0, concat_axis=0, tiled=True)
        return jnp.sum(got.astype(F32), axis=0)
    total = lax.dynamic_index_in_dim(parts, me, 0, keepdims=False).astype(F32)
    for d, perm in enumerate(shifts(axis), 1):
        piece = lax.dynamic_index_in_dim(parts, (me + d) % size, 0, keepdims=False)
        total = total + lax.ppermute(piece, axis, perm).astype(F32)
    return total


def gather_rows(piece, axis):
    size = lax.axis_size(axis)
    me = lax.axis_index(axis)
    rows = piece.shape[0]
    if size > 4:
        return gather_blocks(piece, axis).reshape(size * rows, piece.shape[1])
    whole = jnp.zeros((size * rows, piece.shape[1]), piece.dtype)
    whole = lax.dynamic_update_slice_in_dim(whole, piece, me * rows, 0)
    for d, perm in enumerate(shifts(axis), 1):
        got = lax.ppermute(piece, axis, perm)
        whole = lax.dynamic_update_slice_in_dim(whole, got, ((me - d) % size) * rows, 0)
    return whole


def gather_blocks(piece, axis):
    size = lax.axis_size(axis)
    return lax.all_to_all(
        jnp.broadcast_to(piece[None], (size,) + piece.shape), axis, 0, 0, tiled=True
    )


def core():
    return lax.axis_index("tp") % 2


def layer():
    return lax.axis_index("tp") // 2


def layers():
    return lax.axis_size("tp") // 2


def layer_groups():
    return [[2 * z + c for z in range(layers())] for c in range(2)]


def column_groups():
    members = lax.axis_size("tp")
    return [
        [k * members + 2 * z + c for k in range(lax.axis_size("kv")) for z in range(layers())]
        for c in range(2)
    ]


def swap_cores(x):
    return lax.ppermute(x, "tp", [(s, s ^ 1) for s in range(lax.axis_size("tp"))])


def over_layer(x, d):
    return lax.ppermute(x, "tp", [(s, s ^ (2 * d)) for s in range(lax.axis_size("tp"))])


def both_cores(mine):
    other = swap_cores(mine)
    first = core() == 0
    return jnp.where(first, mine, other), jnp.where(first, other, mine)


def gather_members(piece):
    if layers() > 4:
        return side_by_side(gather_blocks(piece, "tp"))
    got = jnp.zeros((layers(),) + piece.shape, piece.dtype)
    got = lax.dynamic_update_index_in_dim(got, piece, layer(), 0)
    for d in range(1, layers()):
        got = lax.dynamic_update_index_in_dim(got, over_layer(piece, d), layer() ^ d, 0)
    low, high = both_cores(got)
    return side_by_side(jnp.stack([low, high], axis=1).reshape((-1,) + piece.shape))


def sum_members_scattered(parts):
    if layers() > 4:
        got = lax.all_to_all(parts, "tp", 0, 0, tiled=True)
        return jnp.sum(got.astype(F32), axis=0)
    pairs = parts.reshape((layers(), 2) + parts.shape[1:])
    theirs = lax.dynamic_index_in_dim(pairs, 1 - core(), 1, keepdims=False)
    ours = lax.dynamic_index_in_dim(pairs, core(), 1, keepdims=False).astype(F32)
    ours = ours + swap_cores(theirs).astype(F32)
    sent = ours.astype(BF16)
    total = lax.dynamic_index_in_dim(ours, layer(), 0, keepdims=False)
    for d in range(1, layers()):
        piece = lax.dynamic_index_in_dim(sent, layer() ^ d, 0, keepdims=False)
        total = total + over_layer(piece, d).astype(F32)
    return total


def exchange_columns(half):
    groups = lax.axis_size("kv")
    spread = jnp.broadcast_to(
        half[:, None], (groups, layers()) + half.shape[1:]
    ).reshape((groups * layers(),) + half.shape[1:])
    got = lax.all_to_all(spread, ("kv", "tp"), 0, 0, axis_index_groups=column_groups())
    total = jnp.sum(got.reshape((groups, layers()) + half.shape[1:]).astype(F32), axis=1)
    return both_cores(total.astype(BF16))


def side_by_side(blocks):
    count, rows, cols = blocks.shape
    return jnp.transpose(blocks, (1, 0, 2)).reshape(rows, count * cols)


def apart(whole, count):
    rows, cols = whole.shape
    return jnp.transpose(whole.reshape(rows, count, cols // count), (1, 0, 2))


def cuts(extent, count):
    step = extent // count
    if extent % count or step % LANES:
        return [(0, extent)]
    return [(i * step, step) for i in range(count)]


def params():
    return pltpu.CompilerParams(vmem_limit_bytes=48 * 1024 * 1024)


ANY = pl.BlockSpec(memory_space=pl.ANY)
VMEM = pl.BlockSpec(memory_space=pltpu.VMEM)


def gate_up(block, gain_block, w_gate, w_up):
    rows, width = block.shape
    units = w_gate.shape[1]
    pieces = cuts(units, 4)

    def kernel(x_ref, gain_ref, gate_hbm, up_hbm, out_ref, gate_buf, up_buf, sems):
        copies = []
        for i, (at, size) in enumerate(pieces):
            for j, (src, dst) in enumerate(((gate_hbm, gate_buf), (up_hbm, up_buf))):
                copy = pltpu.make_async_copy(
                    src.at[:, pl.ds(at, size)], dst.at[:, pl.ds(at, size)], sems.at[i, j]
                )
                copy.start()
                copies.append((copy, dst, at, size, j * units + at))
        values = x_ref[...].astype(F32)
        scaled = (values * gain_ref[...]).astype(BF16)
        squares = jnp.sum(values * values, axis=1, keepdims=True)
        high = squares.astype(BF16).astype(F32)
        lane = lax.broadcasted_iota(jnp.int32, (rows, LANES), 1)
        tail = jnp.where(lane == 0, high, jnp.where(lane == 1, squares - high, 0.0))
        out_ref[:, pl.ds(2 * units, LANES)] = tail.astype(BF16)
        for copy, buf, at, size, to in copies:
            copy.wait()
            acc = jnp.dot(scaled, buf[:, pl.ds(at, size)], preferred_element_type=F32)
            out_ref[:, pl.ds(to, size)] = acc.astype(BF16)

    return pl.pallas_call(
        kernel,
        out_shape=jax.ShapeDtypeStruct((rows, 2 * units + LANES), BF16),
        in_specs=[VMEM, VMEM, ANY, ANY],
        out_specs=VMEM,
        scratch_shapes=[
            pltpu.VMEM((width, units), BF16),
            pltpu.VMEM((width, units), BF16),
            pltpu.SemaphoreType.DMA((len(pieces), 2)),
        ],
        compiler_params=params(),
        name="gate_up",
    )(block, gain_block, w_gate, w_up)


def down(hidden, w_down, count):
    rows, units = hidden.shape
    width = w_down.shape[1]
    part = width // count
    pieces = cuts(width, 4)

    def kernel(x_ref, w_hbm, out_ref, buf, sems):
        copies = []
        for i, (at, size) in enumerate(pieces):
            copy = pltpu.make_async_copy(
                w_hbm.at[:, pl.ds(at, size)], buf.at[:, pl.ds(at, size)], sems.at[i]
            )
            copy.start()
            copies.append(copy)
        for copy, (at, size) in zip(copies, pieces):
            copy.wait()
            acc = jnp.dot(x_ref[...], buf[:, pl.ds(at, size)], preferred_element_type=F32)
            acc = acc.astype(BF16)
            for off in range(0, size, min(part, size)):
                step = min(part, size)
                out_ref[(at + off) // part, :, pl.ds((at + off) % part, step)] = acc[
                    :, off : off + step
                ]

    return pl.pallas_call(
        kernel,
        out_shape=jax.ShapeDtypeStruct((count, rows, part), BF16),
        in_specs=[VMEM, ANY],
        out_specs=VMEM,
        scratch_shapes=[pltpu.VMEM((units, width), BF16), pltpu.SemaphoreType.DMA((len(pieces),))],
        compiler_params=params(),
        name="down",
    )(hidden, w_down)


def cell(own_rows, gain, w_query, w_key, w_value, w_gates, w_out, bias, memory, normalizer, stabilizer, groups):
    seqs, model = own_rows.shape
    _, heads, dv, dk = memory.shape
    half = model // (2 * groups)
    steps = cuts(model, 4)
    seq_steps = [(i * (seqs // 4), seqs // 4) for i in range(4)] if seqs % 4 == 0 else [(0, seqs)]
    out_steps = cuts(model, 4)

    def kernel(
        x_ref, gain_ref, gates_ref, bias_ref, norm_ref, stab_ref,
        q_hbm, k_hbm, v_hbm, out_hbm, mem_hbm,
        part_ref, key_ref, value_ref, keep_ref, admit_ref, norm_out, stab_out,
        q_buf, k_buf, v_buf, out_buf, mem_buf, w_sems, mem_sems, out_sems,
    ):
        w_copies, mem_copies, out_copies = [], [], []
        for i, (at, size) in enumerate(steps):
            for j, (src, dst) in enumerate(((q_hbm, q_buf), (k_hbm, k_buf), (v_hbm, v_buf))):
                w_copies.append(
                    pltpu.make_async_copy(
                        src.at[pl.ds(at, size)], dst.at[pl.ds(at, size)], w_sems.at[i, j]
                    )
                )
        for i, (at, size) in enumerate(seq_steps):
            mem_copies.append(
                pltpu.make_async_copy(
                    mem_hbm.at[pl.ds(at, size)], mem_buf.at[pl.ds(at, size)], mem_sems.at[i]
                )
            )
        for i, (at, size) in enumerate(out_steps):
            out_copies.append(
                pltpu.make_async_copy(
                    out_hbm.at[:, pl.ds(at, size)], out_buf.at[:, pl.ds(at, size)], out_sems.at[i]
                )
            )
        for copy in w_copies + mem_copies + out_copies:
            copy.start()
        values = x_ref[...].astype(F32)
        scale = lax.rsqrt(jnp.mean(values * values, axis=1, keepdims=True) + EPS)
        cell_in = (values * gain_ref[...]).astype(BF16)
        gates = scale * lax.dot_general(
            cell_in, gates_ref[...], (((1,), (1,)), ((), ())), preferred_element_type=F32
        )
        sums = [0.0, 0.0, 0.0]
        for i, (at, size) in enumerate(steps):
            for j, buf in enumerate((q_buf, k_buf, v_buf)):
                w_copies[3 * i + j].wait()
                sums[j] = sums[j] + jnp.dot(
                    cell_in[:, at : at + size], buf[pl.ds(at, size)], preferred_element_type=F32
                )
        query = scale * sums[0] * dk ** (-0.5)
        key = scale * sums[1]
        value = scale * sums[2]
        key_ref[...] = key
        value_ref[...] = value
        input_pre = gates[:, :heads]
        carried = jax.nn.log_sigmoid(gates[:, heads : 2 * heads] + bias_ref[...]) + stab_ref[...]
        stabil = jnp.maximum(carried, input_pre)
        keep = jnp.exp(carried - stabil)
        admit = jnp.exp(input_pre - stabil)
        stab_out[...] = stabil
        keep_ref[...] = keep
        admit_ref[...] = admit
        norms = norm_ref[...]
        asked = query.astype(BF16)
        recalled = [jnp.zeros((seqs, dv), F32) for _ in range(heads)]
        row = lax.broadcasted_iota(jnp.int32, (seqs, dv), 0)
        for copy, (at, size) in zip(mem_copies, seq_steps):
            copy.wait()
            for b in range(at, at + size):
                for h in range(heads):
                    got = lax.dot_general(
                        asked[:, h * dk : (h + 1) * dk],
                        mem_buf[b, h].astype(BF16),
                        (((1,), (1,)), ((), ())),
                        preferred_element_type=F32,
                    )
                    recalled[h] = jnp.where(row == b, got, recalled[h])
        outs = []
        for h in range(heads):
            lanes = slice(h * dk, (h + 1) * dk)
            q, k, n = query[:, lanes], key[:, lanes], norms[:, lanes]
            kept, let = keep[:, h : h + 1], admit[:, h : h + 1]
            matched = let * jnp.sum(q * k, axis=1, keepdims=True)
            numer = kept * recalled[h] + matched * value[:, h * dv : (h + 1) * dv]
            denom = kept * jnp.sum(n * q, axis=1, keepdims=True) + matched
            outs.append((numer / jnp.maximum(jnp.abs(denom), 1.0)).astype(BF16))
            norm_out[:, pl.ds(h * dk, dk)] = kept * n + let * k
        cell_out = jnp.concatenate(outs, axis=1)
        for copy, (at, size) in zip(out_copies, out_steps):
            copy.wait()
            acc = jnp.dot(cell_out, out_buf[:, pl.ds(at, size)], preferred_element_type=F32)
            acc = acc.astype(BF16)
            for off in range(0, size, half):
                which = (at + off) // half
                part_ref[which % 2, which // 2] = acc[:, off : off + half]

    shape = jax.ShapeDtypeStruct
    return pl.pallas_call(
        kernel,
        out_shape=(
            shape((2, groups, seqs, half), BF16),
            shape((seqs, heads * dk), F32),
            shape((seqs, heads * dv), F32),
            shape((seqs, heads), F32),
            shape((seqs, heads), F32),
            shape((seqs, heads * dk), F32),
            shape((seqs, heads), F32),
        ),
        in_specs=[VMEM] * 6 + [ANY] * 5,
        out_specs=(VMEM,) * 7,
        scratch_shapes=[
            pltpu.VMEM(w_query.shape, BF16),
            pltpu.VMEM(w_key.shape, BF16),
            pltpu.VMEM(w_value.shape, BF16),
            pltpu.VMEM(w_out.shape, BF16),
            pltpu.VMEM(memory.shape, F32),
            pltpu.SemaphoreType.DMA((len(steps), 3)),
            pltpu.SemaphoreType.DMA((len(seq_steps),)),
            pltpu.SemaphoreType.DMA((len(out_steps),)),
        ],
        compiler_params=params(),
        name="cell",
    )(
        own_rows, gain[None], w_gates, bias[None], normalizer.reshape(seqs, heads * dk), stabilizer,
        w_query, w_key, w_value, w_out, memory,
    )


def gated_part(block, gain, w_gate, w_up, w_down, model_width, count):
    groups = lax.axis_size("kv")
    rows, width = block.shape
    units = w_gate.shape[1]
    gain_block = lax.dynamic_slice_in_dim(gain, lax.axis_index("kv") * width, width, 0)
    parts = gate_up(block, gain_block[None], w_gate, w_up).reshape(groups, rows // groups, -1)
    total = sum_rows_scattered(parts, "kv")
    sq = total[:, 2 * units : 2 * units + 1] + total[:, 2 * units + 1 : 2 * units + 2]
    scale = lax.rsqrt(sq / model_width + EPS)
    piece = (jax.nn.silu(scale * total[:, :units]) * (scale * total[:, units : 2 * units])).astype(BF16)
    return down(gather_rows(piece, "kv"), w_down, count)


def body(
    tokens,
    memory,
    normalizer,
    stabilizer,
    first_gain,
    first_gate,
    first_up,
    first_down,
    mixer_gain,
    query_weight,
    key_weight,
    value_weight,
    input_weight,
    forget_weight,
    forget_bias,
    output_weight,
    last_gain,
    last_gate,
    last_up,
    last_down,
):
    model_width = first_gain.shape[0]
    rows, col_width = tokens.shape
    groups, members = lax.axis_size("kv"), lax.axis_size("tp")
    seq_count, head_count, value_size, key_size = memory.shape
    width = members * col_width
    half = width // 2
    leads = (layer() == 0).astype(F32)
    block = gather_members(tokens)
    part = gated_part(block, first_gain, first_gate, first_up, first_down, model_width, 2)
    theirs = lax.dynamic_index_in_dim(part, 1 - core(), 0, keepdims=False)
    ours = lax.dynamic_index_in_dim(part, core(), 0, keepdims=False).astype(F32)
    held = lax.dynamic_slice_in_dim(block, core() * half, half, 1).astype(F32)
    ours = 0.5 * (ours + swap_cores(theirs).astype(F32)) + leads * held
    low, high = exchange_columns(ours.astype(BF16).reshape(groups, seq_count, half))
    own_rows = side_by_side(jnp.concatenate([low, high], axis=2))
    first_head = lax.axis_index("tp") * head_count
    w_gates = jnp.concatenate(
        [
            lax.dynamic_slice_in_dim(input_weight.T, first_head, head_count, 0),
            lax.dynamic_slice_in_dim(forget_weight.T, first_head, head_count, 0),
            jnp.zeros((16 - 2 * head_count, model_width), BF16),
        ],
        axis=0,
    )
    pairs, key, value, keep, admit, new_normalizer, new_stabilizer = cell(
        own_rows, mixer_gain, query_weight, key_weight, value_weight, w_gates, output_weight,
        forget_bias, memory, normalizer, stabilizer, groups,
    )
    theirs = lax.dynamic_index_in_dim(pairs, 1 - core(), 0, keepdims=False)
    ours = lax.dynamic_index_in_dim(pairs, core(), 0, keepdims=False).astype(F32)
    held = lax.dynamic_index_in_dim(
        own_rows.reshape(seq_count, groups, 2, half), core(), 2, keepdims=False
    ).astype(F32)
    ours = ours + swap_cores(theirs).astype(F32) + leads * jnp.transpose(held, (1, 0, 2))
    ours, keep, admit, value, key = lax.optimization_barrier(
        (ours.astype(BF16), keep, admit, value, key)
    )
    low, high = exchange_columns(ours)
    value = value.reshape(seq_count, head_count, value_size, 1)
    key = key.reshape(seq_count, head_count, 1, key_size)
    new_memory = keep[..., None, None] * memory + admit[..., None, None] * value * key
    new_normalizer = new_normalizer.reshape(normalizer.shape)
    whole_two = jnp.concatenate([low, high], axis=2).reshape(rows, width)
    wide = layers() <= 4 and col_width % LANES == 0
    part = gated_part(
        whole_two, last_gain, last_gate, last_up, last_down, model_width, members if wide else 1
    )
    share = sum_members_scattered(part if wide else apart(part[0], members))
    own_columns = lax.dynamic_slice_in_dim(
        whole_two, lax.axis_index("tp") * col_width, col_width, 1
    )
    result = (own_columns.astype(F32) + 0.5 * share).astype(BF16)
    return (result, new_memory, new_normalizer, new_stabilizer)


def solution(mesh):
    in_specs = (
        P(None, ("kv", "tp")),
        P("kv", "tp", None, None),
        P("kv", "tp", None),
        P("kv", "tp"),
        P(),
        P("kv", "tp"),
        P("kv", "tp"),
        P("tp", "kv"),
        P(),
        P(None, "tp"),
        P(None, "tp"),
        P(None, "tp"),
        P(),
        P(),
        P("tp"),
        P("tp", None),
        P(),
        P("kv", "tp"),
        P("kv", "tp"),
        P("tp", "kv"),
    )
    out_specs = (
        P(None, ("kv", "tp")),
        P("kv", "tp", None, None),
        P("kv", "tp", None),
        P("kv", "tp"),
    )
    return jax.shard_map(body, mesh=mesh, in_specs=in_specs, out_specs=out_specs, check_vma=False)
```

time: 143 us -> 120 us (0.84)
  matrix products: 22.8 us -> 0 us
  waiting for transfers between devices: 51.6 us -> 32 us
  Pallas kernels: 0 us -> 17.3 us
  blocking collectives: 0 us -> 13.8 us
  starting transfers between devices: 39.2 us -> 29.6 us
  local copies, waits for them, and re-layouts: 16.9 us -> 14.8 us
    all_to_all x6 -> x1, waiting for transfers between devices: 38.7 us -> 9.9 us  [exchange_columns(): lax.all_to_all(spread, ('kv', 'tp'), 0, 0, axis_index_groups=column_group...]
    dot_general x11 -> x0, matrix products: 22.8 us -> none  [the longest x2 5.1 us: gated_share(): sums = jnp.dot(hidden, w_down, preferred_element_type=F32).astype(BF16)]
    all_to_all x6 -> x1, starting transfers between devices: 22.4 us -> 4.04 us  [exchange_columns(): lax.all_to_all(spread, ('kv', 'tp'), 0, 0, axis_index_groups=column_group...]
    pallas_call x0 -> x5, Pallas kernels: none -> 17.3 us  [the longest x2 6.82 us: gate_up(): pl.pallas_call(kernel, out_shape=jax.ShapeDtypeStruct((rows, 2 * units +...]
    all_to_all x0 -> x1, blocking collectives: none -> 13.8 us  [exchange_columns(): lax.all_to_all(spread, ('kv', 'tp'), 0, 0, axis_index_groups=column_group...]
    ppermute x0 -> x12, starting transfers between devices: none -> 9.77 us  [the longest x6 9.26 us: over_layer(): lax.ppermute(x, 'tp', [(s, s ^ 2 * d) for s in range(lax.axis_size('tp'))])]
    ppermute x0 -> x12, waiting for transfers between devices: none -> 8.62 us  [the longest x6 4.64 us: swap_cores(): lax.ppermute(x, 'tp', [(s, s ^ 1) for s in range(lax.axis_size('tp'))])]
    unnamed x34 -> x41, local copies, waits for them, and re-layouts: 0.74 us -> 6.95 us
  transfers between devices with their start and end apart: 18 -> 25, of which waited for: 17 -> 17; matrix products, arithmetic and copies ran while one was open for 3% -> 11% of each run, Pallas kernels for 0% -> 0%
where the time goes in v2:
time: 120 us; the launch traced here: 119 us
  waiting for transfers between devices  32 us (27%)
  starting transfers between devices  29.6 us (25%)
  Pallas kernels  17.3 us (14%)
  local copies, waits for them, and re-layouts  14.8 us (12%)
  blocking collectives  13.8 us (12%)
  other arithmetic  10.6 us (9%)
  between operations  1.2 us (1%)
    all_to_all x1, blocking collectives, exchange_columns(): lax.all_to_all(spread, ('kv', 'tp'), 0, 0, axis_index_groups=column_group...  13.8 us
    all_to_all x1, waiting for transfers between devices, exchange_columns(): lax.all_to_all(spread, ('kv', 'tp'), 0, 0, axis_index_groups=column_group...  9.9 us
    ppermute x6, starting transfers between devices, over_layer(): lax.ppermute(x, 'tp', [(s, s ^ 2 * d) for s in range(lax.axis_size('tp'))])  9.26 us
    ppermute x6, waiting for transfers between devices, sum_rows_scattered(): total = total + lax.ppermute(piece, axis, perm).astype(F32)  8.62 us
    ppermute x6, starting transfers between devices, sum_rows_scattered(): total = total + lax.ppermute(piece, axis, perm).astype(F32)  7.92 us
    ppermute x6, starting transfers between devices, gather_rows(): got = lax.ppermute(piece, axis, perm)  7.88 us
    unnamed x41, local copies, waits for them, and re-layouts  6.95 us
    pallas_call x2, Pallas kernels, gate_up(): pl.pallas_call(kernel, out_shape=jax.ShapeDtypeStruct((rows, 2 * units +...  6.82 us
  transfers between devices with their start and end apart: 25, of which 17 were waited for; matrix products, arithmetic and copies ran while one was open for 11% of the time, Pallas kernels for 0%

profile of v2, /device:TPU:0, one launch (start us, length us, event | category | flops | bytes accessed | tf_op | source)
XLA Modules:
  0.0 119.3 jit_solution(12563901376990147664)
XLA Ops:
  0.6 3.1 %collective-permute-start = (bf16[64,128]{1,0:T(8,128)(2,1)}, bf16[64,128]{1,0:T(8,128)(2,1)S(1)}, u32[]{:S(2)}, u32[]{:S(2)}) collective-permute-start(bf16[64,128]{1,0:T(8,128)(2,1)} %param.20), channel_id=1, source_target_pairs={{0,2},{1,3},{2,0},{3,1},{4,6},{5,7},{6,4},{7,5},{8,10},{9,11},{10,... | collective-permute-start | bytes 49160 | tf_op jit(solution)/shard_map/ppermute | solution.py:82
  3.7 2.5 %collective-permute-start.2 = (bf16[64,128]{1,0:T(8,128)(2,1)}, bf16[64,128]{1,0:T(8,128)(2,1)S(1)}, u32[]{:S(2)}, u32[]{:S(2)}) collective-permute-start(bf16[64,128]{1,0:T(8,128)(2,1)} %param.20), channel_id=1, source_target_pairs={{0,6},{1,7},{2,4},{3,5},{4,2},{5,3},{6,0},{7,1},{8,14},{9,15},{10,... | collective-permute-start | bytes 49160 | tf_op jit(solution)/shard_map/ppermute | solution.py:82
  7.1 4.0 %collective-permute-done.1 = bf16[64,128]{1,0:T(8,128)(2,1)S(1)} collective-permute-done((bf16[64,128]{1,0:T(8,128)(2,1)}, bf16[64,128]{1,0:T(8,128)(2,1)S(1)}, u32[]{:S(2)}, u32[]{:S(2)}) %collective-permute-start.1) | collective-permute-done | bytes 16416 | tf_op jit(solution)/shard_map/ppermute | solution.py:82
  12.5 1.9 %copy-done = bf16[1024,1536]{1,0:T(8,128)(2,1)S(1)} copy-done((bf16[1024,1536]{1,0:T(8,128)(2,1)S(1)}, bf16[1024,1536]{1,0:T(8,128)(2,1)}, u32[]{:S(2)}) %copy-start) | copy-done | bytes 3145752
  14.5 3.4 %gate_up.2 = bf16[64,3200]{1,0:T(8,128)(2,1)S(1)} custom-call(bf16[64,1024]{1,0:T(8,128)(2,1)S(1)} %bitcast.111, f32[1,1024]{1,0:T(1,128)S(1)} %bitcast.120, bf16[1024,1536]{1,0:T(8,128)(2,1)S(1)} %copy-done, bf16[1024,1536]{1,0:T(8,128)(2,1)} %up_hbm.2), custom_call_target="tpu_custom_call" | custom-call | tf_op jit(solution)/shard_map/gate_up/pallas_call | solution.py:179
  18.6 1.5 %collective-permute-start.4 = (bf16[16,3200]{1,0:T(8,128)(2,1)}, bf16[16,3200]{1,0:T(8,128)(2,1)}, u32[]{:S(2)}, u32[]{:S(2)}) collective-permute-start(bf16[16,3200]{1,0:T(8,128)(2,1)} %get-tuple-element.53), channel_id=1, source_target_pairs={{0,8},{8,16},{16,24},{24,0},{1,9},{9,17},{17,25},{25,1},{2,10},{10... | collective-permute-start | bytes 307208 | tf_op jit(solution)/shard_map/ppermute | solution.py:28
  20.1 1.4 %collective-permute-start.6 = (bf16[16,3200]{1,0:T(8,128)(2,1)}, bf16[16,3200]{1,0:T(8,128)(2,1)}, u32[]{:S(2)}, u32[]{:S(2)}) collective-permute-start(bf16[16,3200]{1,0:T(8,128)(2,1)} %get-tuple-element.54), channel_id=1, source_target_pairs={{0,24},{8,0},{16,8},{24,16},{1,25},{9,1},{17,9},{25,17},{2,26},{10... | collective-permute-start | bytes 307208 | tf_op jit(solution)/shard_map/ppermute | solution.py:28
  21.5 1.5 %collective-permute-start.5 = (bf16[16,3200]{1,0:T(8,128)(2,1)}, bf16[16,3200]{1,0:T(8,128)(2,1)}, u32[]{:S(2)}, u32[]{:S(2)}) collective-permute-start(bf16[16,3200]{1,0:T(8,128)(2,1)} %get-tuple-element.55), channel_id=1, source_target_pairs={{0,16},{8,24},{16,0},{24,8},{1,17},{9,25},{17,1},{25,9},{2,18},{10... | collective-permute-start | bytes 307208 | tf_op jit(solution)/shard_map/ppermute | solution.py:28
  23.1 2.5 %collective-permute-done.4 = bf16[16,3200]{1,0:T(8,128)(2,1)} collective-permute-done((bf16[16,3200]{1,0:T(8,128)(2,1)}, bf16[16,3200]{1,0:T(8,128)(2,1)}, u32[]{:S(2)}, u32[]{:S(2)}) %collective-permute-start.4) | collective-permute-done | bytes 102432 | tf_op jit(solution)/shard_map/ppermute | solution.py:28
  25.6 1.4 %collective-permute-done.6 = bf16[16,3200]{1,0:T(8,128)(2,1)} collective-permute-done((bf16[16,3200]{1,0:T(8,128)(2,1)}, bf16[16,3200]{1,0:T(8,128)(2,1)}, u32[]{:S(2)}, u32[]{:S(2)}) %collective-permute-start.6) | collective-permute-done | bytes 102432 | tf_op jit(solution)/shard_map/ppermute | solution.py:28
  29.1 2.0 %collective-permute-start.7 = (bf16[16,1536]{1,0:T(8,128)(2,1)}, bf16[16,1536]{1,0:T(8,128)(2,1)}, u32[]{:S(2)}, u32[]{:S(2)}) collective-permute-start(bf16[16,1536]{1,0:T(8,128)(2,1)} %get-tuple-element.49), channel_id=1, source_target_pairs={{0,8},{8,16},{16,24},{24,0},{1,9},{9,17},{17,25},{25,1},{2,10},{10... | collective-permute-start | bytes 147464 | tf_op jit(solution)/shard_map/ppermute | solution.py:41
  31.1 1.4 %collective-permute-start.8 = (bf16[16,1536]{1,0:T(8,128)(2,1)}, bf16[16,1536]{1,0:T(8,128)(2,1)S(1)}, u32[]{:S(2)}, u32[]{:S(2)}) collective-permute-start(bf16[16,1536]{1,0:T(8,128)(2,1)} %get-tuple-element.49), channel_id=1, source_target_pairs={{0,16},{8,24},{16,0},{24,8},{1,17},{9,25},{17,1},{25,9},{2,18},{10... | collective-permute-start | bytes 147464 | tf_op jit(solution)/shard_map/ppermute | solution.py:41
  33.5 1.2 %collective-permute-done.7 = bf16[16,1536]{1,0:T(8,128)(2,1)} collective-permute-done((bf16[16,1536]{1,0:T(8,128)(2,1)}, bf16[16,1536]{1,0:T(8,128)(2,1)}, u32[]{:S(2)}, u32[]{:S(2)}) %collective-permute-start.7) | collective-permute-done | bytes 49184 | tf_op jit(solution)/shard_map/ppermute | solution.py:41
  35.6 1.3 %collective-permute-done.9 = bf16[16,1536]{1,0:T(8,128)(2,1)S(1)} collective-permute-done((bf16[16,1536]{1,0:T(8,128)(2,1)}, bf16[16,1536]{1,0:T(8,128)(2,1)S(1)}, u32[]{:S(2)}, u32[]{:S(2)}) %collective-permute-start.9) | collective-permute-done | bytes 49184 | tf_op jit(solution)/shard_map/ppermute | solution.py:41
  36.8 1.9 %down.2 = bf16[2,64,512]{2,1,0:T(8,128)(2,1)S(1)} custom-call(bf16[64,1536]{1,0:T(8,128)(2,1)S(1)} %constant_dynamic-update-slice_fusion.4.x_ref, bf16[1536,1024]{1,0:T(8,128)(2,1)S(1)} %copy-done.2), custom_call_target="tpu_custom_call" | custom-call | tf_op jit(solution)/shard_map/down/pallas_call | solution.py:218
  39.4 1.2 %collective-permute-done.10 = bf16[64,512]{1,0:T(8,128)(2,1)S(1)} collective-permute-done((bf16[64,512]{1,0:T(8,128)(2,1)S(1)}, bf16[64,512]{1,0:T(8,128)(2,1)S(1)}, u32[]{:S(2)}, u32[]{:S(2)}) %collective-permute-start.10) | collective-permute-done | bytes 65568 | tf_op jit(solution)/shard_map/ppermute | solution.py:78
  42.3 4.0 %all-to-all-start = ((bf16[16,16,512]{2,1,0:T(8,128)(2,1)}), bf16[16,16,512]{2,1,0:T(8,128)(2,1)S(1)}, u32[]{:S(2)}, u32[]{:S(2)}) async-start(bf16[16,16,512]{2,1,0:T(8,128)(2,1)} %bitcast.17), calls=%async_computation | async-start | bytes 524288 | tf_op jit(solution)/shard_map/all_to_all | solution.py:123
  47.3 9.9 %all-to-all-done = bf16[16,16,512]{2,1,0:T(8,128)(2,1)S(1)} async-done(((bf16[16,16,512]{2,1,0:T(8,128)(2,1)}), bf16[16,16,512]{2,1,0:T(8,128)(2,1)S(1)}, u32[]{:S(2)}, u32[]{:S(2)}) %all-to-all-start) | async-done | bytes 262176 | tf_op jit(solution)/shard_map/all_to_all | solution.py:123
  58.8 1.6 %copy-done.5 = bf16[4096,256]{1,0:T(8,128)(2,1)S(1)} copy-done((bf16[4096,256]{1,0:T(8,128)(2,1)S(1)}, bf16[4096,256]{1,0:T(8,128)(2,1)}, u32[]{:S(2)}) %copy-start.5) | copy-done | bytes 2097176
  61.0 6.8 %cell.1 = (bf16[2,4,16,512]{3,2,1,0:T(8,128)(2,1)S(1)}, f32[16,256]{1,0:T(8,128)S(1)}, f32[16,512]{1,0:T(8,128)S(1)}, f32[16,2]{1,0:T(8,128)S(1)}, f32[16,2]{1,0...) custom-call(bf16[16,4096]{1,0:T(8,128)(2,1)S(1)} %bitcast.115, f32[1,4096]{1,0:T(1,128)S(1)} %bitcast.119, ...), custom_call_target="tpu_custom_call" | custom-call | tf_op jit(solution)/shard_map/cell/pallas_call | solution.py:326
  69.2 13.8 %all_to_all.10 = bf16[16,16,512]{2,1,0:T(8,128)(2,1)S(1)} all-to-all(bf16[16,16,512]{2,1,0:T(8,128)(2,1)S(1)} %bitcast.123), channel_id=1, replica_groups={{0,2,4,6,8,10,12,14,16,18,20,22,24,26,28,30},{1,3,5,7,9,11,13,15,17,19,..., dimensions={0} | all-to-all | bytes 524288 | tf_op jit(solution)/shard_map/all_to_all | solution.py:123
  84.4 3.4 %gate_up.3 = bf16[64,3200]{1,0:T(8,128)(2,1)S(1)} custom-call(bf16[64,1024]{1,0:T(8,128)(2,1)S(1)} %bitcast.113, f32[1,1024]{1,0:T(1,128)S(1)} %bitcast.121, bf16[1024,1536]{1,0:T(8,128)(2,1)S(1)} %copy-done.1, bf16[1024,1536]{1,0:T(8,128)(2,1)} %up_hbm.3), custom_call_target="tpu_custom_call" | custom-call | tf_op jit(solution)/shard_map/gate_up/pallas_call | solution.py:179
  88.0 2.9 %collective-permute-start.16 = (bf16[16,3200]{1,0:T(8,128)(2,1)S(1)}, bf16[16,3200]{1,0:T(8,128)(2,1)S(1)}, u32[]{:S(2)}, u32[]{:S(2)}) collective-permute-start(bf16[16,3200]{1,0:T(8,128)(2,1)S(1)} %get-tuple-element.51), channel_id=1, source_target_pairs={{0,24},{8,0},{16,8},{24,16},{1,25},{9,1},{17,9},{25,17},{2,26},{10... | collective-permute-start | bytes 307208 | tf_op jit(solution)/shard_map/ppermute | solution.py:28
  91.4 3.2 %collective-permute-done.14 = bf16[16,3200]{1,0:T(8,128)(2,1)S(1)} collective-permute-done((bf16[16,3200]{1,0:T(8,128)(2,1)S(1)}, bf16[16,3200]{1,0:T(8,128)(2,1)S(1)}, u32[]{:S(2)}, u32[]{:S(2)}) %collective-permute-start.14) | collective-permute-done | bytes 102432 | tf_op jit(solution)/shard_map/ppermute | solution.py:28
  97.9 1.3 %copy.43 = f32[16,2]{0,1:T(2,128)} copy(f32[16,2]{1,0:T(8,128)} %copy-done.15) | data formatting | bytes 256
  100.5 1.4 %collective-permute-start.18 = (bf16[16,1536]{1,0:T(8,128)(2,1)}, bf16[16,1536]{1,0:T(8,128)(2,1)S(1)}, u32[]{:S(2)}, u32[]{:S(2)}) collective-permute-start(bf16[16,1536]{1,0:T(8,128)(2,1)} %get-tuple-element.47), channel_id=1, source_target_pairs={{0,16},{8,24},{16,0},{24,8},{1,17},{9,25},{17,1},{25,9},{2,18},{10... | collective-permute-start | bytes 147464 | tf_op jit(solution)/shard_map/ppermute | solution.py:41
  101.9 1.2 collective-permute-start.19
  104.8 1.4 %collective-permute-done.19 = bf16[16,1536]{1,0:T(8,128)(2,1)S(1)} collective-permute-done((bf16[16,1536]{1,0:T(8,128)(2,1)}, bf16[16,1536]{1,0:T(8,128)(2,1)S(1)}, u32[]{:S(2)}, u32[]{:S(2)}) %collective-permute-start.19) | collective-permute-done | bytes 49184 | tf_op jit(solution)/shard_map/ppermute | solution.py:41
  106.2 1.9 %down.3 = bf16[8,64,128]{2,1,0:T(8,128)(2,1)S(1)} custom-call(bf16[64,1536]{1,0:T(8,128)(2,1)S(1)} %constant_dynamic-update-slice_fusion.x_ref, bf16[1536,1024]{1,0:T(8,128)(2,1)S(1)} %copy-done.3), custom_call_target="tpu_custom_call" | custom-call | tf_op jit(solution)/shard_map/down/pallas_call | solution.py:218
  111.0 1.1 collective-permute-start.23
  112.1 2.3 %collective-permute-start.22 = (bf16[64,128]{1,0:T(8,128)(2,1)S(1)}, bf16[64,128]{1,0:T(8,128)(2,1)S(1)}, u32[]{:S(2)}, u32[]{:S(2)}) collective-permute-start(bf16[64,128]{1,0:T(8,128)(2,1)S(1)} %get-tuple-element.66), channel_id=1, source_target_pairs={{0,4},{1,5},{2,6},{3,7},{4,0},{5,1},{6,2},{7,3},{8,12},{9,13},{10,... | collective-permute-start | bytes 49160 | tf_op jit(solution)/shard_map/ppermute | solution.py:82
  114.4 4.2 %multiply_add_fusion = f32[16,2,256,128]{3,2,1,0:T(8,128)} fusion(f32[16,2,256,128]{3,2,1,0:T(8,128)} %mem_hbm.1, f32[16,2,128]{2,1,0:T(2,128)S(1)} %mul.175, f32[16,2,256]{2,1,0:T(2,128)S(1)} %broadcast_multiply_fusion, f32[16,2]{1,0:T(8,128)S(1)} %copy-done.12), kind=kLoop, calls=%fused_computation | loop fusion | flops 3145728 | bytes 8437888 | tf_op jit(solution)/shard_map/add | solution.py:432
  (120 shorter events, 25.4 us)
Async XLA Ops:
  0.6 6.5 %collective-permute-start = (bf16[64,128]{1,0:T(8,128)(2,1)}, bf16[64,128]{1,0:T(8,128)(2,1)S(1)}, u32[]{:S(2)}, u32[]{:S(2)}) collective-permute-start(bf16[64,128]{1,0:T(8,128)(2,1)} %param.20), channel_id=1, source_target_pairs={{0,2},{1,3},{2,0},{3,1},{4,6},{5,7},{6,4},{7,5},{8,10},{9,11},{10,... | collective-permute-start | bytes 49160 | tf_op jit(solution)/shard_map/ppermute | solution.py:82
  3.7 7.3 %collective-permute-start.2 = (bf16[64,128]{1,0:T(8,128)(2,1)}, bf16[64,128]{1,0:T(8,128)(2,1)S(1)}, u32[]{:S(2)}, u32[]{:S(2)}) collective-permute-start(bf16[64,128]{1,0:T(8,128)(2,1)} %param.20), channel_id=1, source_target_pairs={{0,6},{1,7},{2,4},{3,5},{4,2},{5,3},{6,0},{7,1},{8,14},{9,15},{10,... | collective-permute-start | bytes 49160 | tf_op jit(solution)/shard_map/ppermute | solution.py:82
  6.2 4.9 %collective-permute-start.1 = (bf16[64,128]{1,0:T(8,128)(2,1)}, bf16[64,128]{1,0:T(8,128)(2,1)S(1)}, u32[]{:S(2)}, u32[]{:S(2)}) collective-permute-start(bf16[64,128]{1,0:T(8,128)(2,1)} %param.20), channel_id=1, source_target_pairs={{0,4},{1,5},{2,6},{3,7},{4,0},{5,1},{6,2},{7,3},{8,12},{9,13},{10,... | collective-permute-start | bytes 49160 | tf_op jit(solution)/shard_map/ppermute | solution.py:82
  11.1 1.3 %collective-permute-start.3 = (bf16[4,64,128]{2,1,0:T(8,128)(2,1)S(1)}, bf16[4,64,128]{2,1,0:T(8,128)(2,1)S(1)}, u32[]{:S(2)}, u32[]{:S(2)}) collective-permute-start(bf16[4,64,128]{2,1,0:T(8,128)(2,1)S(1)} %bitcast_dynamic-update-slice_fusion), channel_id=1, source_target_pairs={{0,1},{1,0},{2,3},{3,2},{4,5},{5,4},{6,7},{7,6},{8,9},{9,8},{10,11... | collective-permute-start | bytes 196616 | tf_op jit(solution)/shard_map/ppermute | solution.py:78
  14.5 22.4 %copy-start.2 = (bf16[1536,1024]{1,0:T(8,128)(2,1)S(1)}, bf16[1536,1024]{1,0:T(8,128)(2,1)}, u32[]{:S(2)}) copy-start(bf16[1536,1024]{1,0:T(8,128)(2,1)} %w_hbm.2) | copy-start | bytes 9437188
  18.6 7.0 %collective-permute-start.4 = (bf16[16,3200]{1,0:T(8,128)(2,1)}, bf16[16,3200]{1,0:T(8,128)(2,1)}, u32[]{:S(2)}, u32[]{:S(2)}) collective-permute-start(bf16[16,3200]{1,0:T(8,128)(2,1)} %get-tuple-element.53), channel_id=1, source_target_pairs={{0,8},{8,16},{16,24},{24,0},{1,9},{9,17},{17,25},{25,1},{2,10},{10... | collective-permute-start | bytes 307208 | tf_op jit(solution)/shard_map/ppermute | solution.py:28
  20.1 6.9 %collective-permute-start.6 = (bf16[16,3200]{1,0:T(8,128)(2,1)}, bf16[16,3200]{1,0:T(8,128)(2,1)}, u32[]{:S(2)}, u32[]{:S(2)}) collective-permute-start(bf16[16,3200]{1,0:T(8,128)(2,1)} %get-tuple-element.54), channel_id=1, source_target_pairs={{0,24},{8,0},{16,8},{24,16},{1,25},{9,1},{17,9},{25,17},{2,26},{10... | collective-permute-start | bytes 307208 | tf_op jit(solution)/shard_map/ppermute | solution.py:28
  21.5 5.5 %collective-permute-start.5 = (bf16[16,3200]{1,0:T(8,128)(2,1)}, bf16[16,3200]{1,0:T(8,128)(2,1)}, u32[]{:S(2)}, u32[]{:S(2)}) collective-permute-start(bf16[16,3200]{1,0:T(8,128)(2,1)} %get-tuple-element.55), channel_id=1, source_target_pairs={{0,16},{8,24},{16,0},{24,8},{1,17},{9,25},{17,1},{25,9},{2,18},{10... | collective-permute-start | bytes 307208 | tf_op jit(solution)/shard_map/ppermute | solution.py:28
  28.1 29.3 %copy-start.18 = (f32[16,2]{0,1:T(2,128)S(1)}, f32[16,2]{0,1:T(2,128)}, u32[]{:S(2)}) copy-start(f32[16,2]{0,1:T(2,128)} %param.23) | copy-start | bytes 388
  28.1 29.4 %copy-start.17 = (f32[16,2,128]{2,1,0:T(2,128)S(1)}, f32[16,2,128]{2,1,0:T(2,128)}, u32[]{:S(2)}) copy-start(f32[16,2,128]{2,1,0:T(2,128)} %param.22) | copy-start | bytes 49156
  28.1 30.6 %copy-start.10 = (f32[4096]{0:T(1024)S(1)}, f32[4096]{0:T(1024)}, u32[]{:S(2)}) copy-start(f32[4096]{0:T(1024)} %param.28) | copy-start | bytes 49156
  29.1 5.7 %collective-permute-start.7 = (bf16[16,1536]{1,0:T(8,128)(2,1)}, bf16[16,1536]{1,0:T(8,128)(2,1)}, u32[]{:S(2)}, u32[]{:S(2)}) collective-permute-start(bf16[16,1536]{1,0:T(8,128)(2,1)} %get-tuple-element.49), channel_id=1, source_target_pairs={{0,8},{8,16},{16,24},{24,0},{1,9},{9,17},{17,25},{25,1},{2,10},{10... | collective-permute-start | bytes 147464 | tf_op jit(solution)/shard_map/ppermute | solution.py:41
  31.1 4.4 %collective-permute-start.8 = (bf16[16,1536]{1,0:T(8,128)(2,1)}, bf16[16,1536]{1,0:T(8,128)(2,1)S(1)}, u32[]{:S(2)}, u32[]{:S(2)}) collective-permute-start(bf16[16,1536]{1,0:T(8,128)(2,1)} %get-tuple-element.49), channel_id=1, source_target_pairs={{0,16},{8,24},{16,0},{24,8},{1,17},{9,25},{17,1},{25,9},{2,18},{10... | collective-permute-start | bytes 147464 | tf_op jit(solution)/shard_map/ppermute | solution.py:41
  32.5 4.3 %collective-permute-start.9 = (bf16[16,1536]{1,0:T(8,128)(2,1)}, bf16[16,1536]{1,0:T(8,128)(2,1)S(1)}, u32[]{:S(2)}, u32[]{:S(2)}) collective-permute-start(bf16[16,1536]{1,0:T(8,128)(2,1)} %get-tuple-element.49), channel_id=1, source_target_pairs={{0,24},{8,0},{16,8},{24,16},{1,25},{9,1},{17,9},{25,17},{2,26},{10... | collective-permute-start | bytes 147464 | tf_op jit(solution)/shard_map/ppermute | solution.py:41
  39.3 1.3 %collective-permute-start.10 = (bf16[64,512]{1,0:T(8,128)(2,1)S(1)}, bf16[64,512]{1,0:T(8,128)(2,1)S(1)}, u32[]{:S(2)}, u32[]{:S(2)}) collective-permute-start(bf16[64,512]{1,0:T(8,128)(2,1)S(1)} %dynamic-slice_bitcast_fusion.8), channel_id=1, source_target_pairs={{0,1},{1,0},{2,3},{3,2},{4,5},{5,4},{6,7},{7,6},{8,9},{9,8},{10,11... | collective-permute-start | bytes 196616 | tf_op jit(solution)/shard_map/ppermute | solution.py:78
  42.3 14.9 %all-to-all-start = ((bf16[16,16,512]{2,1,0:T(8,128)(2,1)}), bf16[16,16,512]{2,1,0:T(8,128)(2,1)S(1)}, u32[]{:S(2)}, u32[]{:S(2)}) async-start(bf16[16,16,512]{2,1,0:T(8,128)(2,1)} %bitcast.17), calls=%async_computation | async-start | bytes 524288 | tf_op jit(solution)/shard_map/all_to_all | solution.py:123
  57.3 1.3 %collective-permute-start.11 = (bf16[4,16,512]{2,1,0:T(8,128)(2,1)S(1)}, bf16[4,16,512]{2,1,0:T(8,128)(2,1)S(1)}, u32[]{:S(2)}, u32[]{:S(2)}) collective-permute-start(bf16[4,16,512]{2,1,0:T(8,128)(2,1)S(1)} %bitcast_reduce_fusion.1), channel_id=1, source_target_pairs={{0,1},{1,0},{2,3},{3,2},{4,5},{5,4},{6,7},{7,6},{8,9},{9,8},{10,11... | collective-permute-start | bytes 196616 | tf_op jit(solution)/shard_map/ppermute | solution.py:78
  61.0 23.4 %copy-start.1 = (bf16[1024,1536]{1,0:T(8,128)(2,1)S(1)}, bf16[1024,1536]{1,0:T(8,128)(2,1)}, u32[]{:S(2)}) copy-start(bf16[1024,1536]{1,0:T(8,128)(2,1)} %gate_hbm.3) | copy-start | bytes 9437188
  67.8 29.2 %copy-start.15 = (f32[16,2]{1,0:T(8,128)}, f32[16,2]{1,0:T(8,128)S(1)}, u32[]{:S(2)}) copy-start(f32[16,2]{1,0:T(8,128)S(1)} %get-tuple-element.43) | copy-start | bytes 388
  67.8 1.3 %collective-permute-start.12 = (bf16[4,16,512]{2,1,0:T(8,128)(2,1)S(1)}, bf16[4,16,512]{2,1,0:T(8,128)(2,1)S(1)}, u32[]{:S(2)}, u32[]{:S(2)}) collective-permute-start(bf16[4,16,512]{2,1,0:T(8,128)(2,1)S(1)} %dynamic-slice_bitcast_fusion.7), channel_id=1, source_target_pairs={{0,1},{1,0},{2,3},{3,2},{4,5},{5,4},{6,7},{7,6},{8,9},{9,8},{10,11... | collective-permute-start | bytes 196616 | tf_op jit(solution)/shard_map/ppermute | solution.py:78
  83.0 1.3 %collective-permute-start.13 = (bf16[4,16,512]{2,1,0:T(8,128)(2,1)S(1)}, bf16[4,16,512]{2,1,0:T(8,128)(2,1)S(1)}, u32[]{:S(2)}, u32[]{:S(2)}) collective-permute-start(bf16[4,16,512]{2,1,0:T(8,128)(2,1)S(1)} %bitcast_reduce_fusion), channel_id=1, source_target_pairs={{0,1},{1,0},{2,3},{3,2},{4,5},{5,4},{6,7},{7,6},{8,9},{9,8},{10,11... | collective-permute-start | bytes 196616 | tf_op jit(solution)/shard_map/ppermute | solution.py:78
  87.8 26.6 %copy-start.12 = (f32[16,2]{1,0:T(8,128)S(1)}, f32[16,2]{1,0:T(8,128)}, u32[]{:S(2)}) copy-start(f32[16,2]{1,0:T(8,128)} %copy-done.11) | copy-start | bytes 388
  87.9 6.7 %collective-permute-start.14 = (bf16[16,3200]{1,0:T(8,128)(2,1)S(1)}, bf16[16,3200]{1,0:T(8,128)(2,1)S(1)}, u32[]{:S(2)}, u32[]{:S(2)}) collective-permute-start(bf16[16,3200]{1,0:T(8,128)(2,1)S(1)} %get-tuple-element.50), channel_id=1, source_target_pairs={{0,8},{8,16},{16,24},{24,0},{1,9},{9,17},{17,25},{25,1},{2,10},{10... | collective-permute-start | bytes 307208 | tf_op jit(solution)/shard_map/ppermute | solution.py:28
  88.0 7.1 %collective-permute-start.16 = (bf16[16,3200]{1,0:T(8,128)(2,1)S(1)}, bf16[16,3200]{1,0:T(8,128)(2,1)S(1)}, u32[]{:S(2)}, u32[]{:S(2)}) collective-permute-start(bf16[16,3200]{1,0:T(8,128)(2,1)S(1)} %get-tuple-element.51), channel_id=1, source_target_pairs={{0,24},{8,0},{16,8},{24,16},{1,25},{9,1},{17,9},{25,17},{2,26},{10... | collective-permute-start | bytes 307208 | tf_op jit(solution)/shard_map/ppermute | solution.py:28
  90.9 5.2 %collective-permute-start.15 = (bf16[16,3200]{1,0:T(8,128)(2,1)S(1)}, bf16[16,3200]{1,0:T(8,128)(2,1)S(1)}, u32[]{:S(2)}, u32[]{:S(2)}) collective-permute-start(bf16[16,3200]{1,0:T(8,128)(2,1)S(1)} %get-tuple-element.52), channel_id=1, source_target_pairs={{0,16},{8,24},{16,0},{24,8},{1,17},{9,25},{17,1},{25,9},{2,18},{10... | collective-permute-start | bytes 307208 | tf_op jit(solution)/shard_map/ppermute | solution.py:28
  97.0 6.0 %collective-permute-start.17 = (bf16[16,1536]{1,0:T(8,128)(2,1)}, bf16[16,1536]{1,0:T(8,128)(2,1)}, u32[]{:S(2)}, u32[]{:S(2)}) collective-permute-start(bf16[16,1536]{1,0:T(8,128)(2,1)} %get-tuple-element.47), channel_id=1, source_target_pairs={{0,8},{8,16},{16,24},{24,0},{1,9},{9,17},{17,25},{25,1},{2,10},{10... | collective-permute-start | bytes 147464 | tf_op jit(solution)/shard_map/ppermute | solution.py:41
  100.5 4.3 %collective-permute-start.18 = (bf16[16,1536]{1,0:T(8,128)(2,1)}, bf16[16,1536]{1,0:T(8,128)(2,1)S(1)}, u32[]{:S(2)}, u32[]{:S(2)}) collective-permute-start(bf16[16,1536]{1,0:T(8,128)(2,1)} %get-tuple-element.47), channel_id=1, source_target_pairs={{0,16},{8,24},{16,0},{24,8},{1,17},{9,25},{17,1},{25,9},{2,18},{10... | collective-permute-start | bytes 147464 | tf_op jit(solution)/shard_map/ppermute | solution.py:41
  101.9 4.3 %collective-permute-start.19 = (bf16[16,1536]{1,0:T(8,128)(2,1)}, bf16[16,1536]{1,0:T(8,128)(2,1)S(1)}, u32[]{:S(2)}, u32[]{:S(2)}) collective-permute-start(bf16[16,1536]{1,0:T(8,128)(2,1)} %get-tuple-element.47), channel_id=1, source_target_pairs={{0,24},{8,0},{16,8},{24,16},{1,25},{9,1},{17,9},{25,17},{2,26},{10... | collective-permute-start | bytes 147464 | tf_op jit(solution)/shard_map/ppermute | solution.py:41
  108.7 1.3 %collective-permute-start.20 = (bf16[4,64,128]{2,1,0:T(8,128)(2,1)S(1)}, bf16[4,64,128]{2,1,0:T(8,128)(2,1)S(1)}, u32[]{:S(2)}, u32[]{:S(2)}) collective-permute-start(bf16[4,64,128]{2,1,0:T(8,128)(2,1)S(1)} %dynamic-slice_bitcast_fusion.6), channel_id=1, source_target_pairs={{0,1},{1,0},{2,3},{3,2},{4,5},{5,4},{6,7},{7,6},{8,9},{9,8},{10,11... | collective-permute-start | bytes 196616 | tf_op jit(solution)/shard_map/ppermute | solution.py:78
  110.9 7.8 %collective-permute-start.21 = (bf16[64,128]{1,0:T(8,128)(2,1)S(1)}, bf16[64,128]{1,0:T(8,128)(2,1)S(1)}, u32[]{:S(2)}, u32[]{:S(2)}) collective-permute-start(bf16[64,128]{1,0:T(8,128)(2,1)S(1)} %get-tuple-element.64), channel_id=1, source_target_pairs={{0,2},{1,3},{2,0},{3,1},{4,6},{5,7},{6,4},{7,5},{8,10},{9,11},{10,... | collective-permute-start | bytes 49160 | tf_op jit(solution)/shard_map/ppermute | solution.py:82
  111.0 7.7 %collective-permute-start.23 = (bf16[64,128]{1,0:T(8,128)(2,1)S(1)}, bf16[64,128]{1,0:T(8,128)(2,1)S(1)}, u32[]{:S(2)}, u32[]{:S(2)}) collective-permute-start(bf16[64,128]{1,0:T(8,128)(2,1)S(1)} %get-tuple-element.65), channel_id=1, source_target_pairs={{0,6},{1,7},{2,4},{3,5},{4,2},{5,3},{6,0},{7,1},{8,14},{9,15},{10,... | collective-permute-start | bytes 49160 | tf_op jit(solution)/shard_map/ppermute | solution.py:82
  112.1 6.6 %collective-permute-start.22 = (bf16[64,128]{1,0:T(8,128)(2,1)S(1)}, bf16[64,128]{1,0:T(8,128)(2,1)S(1)}, u32[]{:S(2)}, u32[]{:S(2)}) collective-permute-start(bf16[64,128]{1,0:T(8,128)(2,1)S(1)} %get-tuple-element.66), channel_id=1, source_target_pairs={{0,4},{1,5},{2,6},{3,7},{4,0},{5,1},{6,2},{7,3},{8,12},{9,13},{10,... | collective-permute-start | bytes 49160 | tf_op jit(solution)/shard_map/ppermute | solution.py:82
  (12 other events, 125.7 us)
